TPU v7x, 32 devices: a whole 2x2x4 slice. The times are simulated.
32 devices in a mesh: ep: 8 (over z, x), tp: 4 (over y, core).
Axes of the slice: x: 2, y: 2, z: 4, core: 2. Of those that a mesh axis runs over, the one named last changes fastest.
Arguments:
- tokens_first: bfloat16 [4096, 2048], P('ep'), may hold values from -6 to 6
- attn_gain: float32 [2048], replicated, may hold values from 0.1 to 1.9
- w_query: bfloat16 [2048, 1024], P(None, 'tp'), may hold values from -6 to 6
- key_matrix: bfloat16 [2048, 512], P(None, 'tp'), may hold values from -6 to 6
- value_matrix: bfloat16 [2048, 512], P(None, 'tp'), may hold values from -0.125 to 0.125
- head_sink_logit: float32 [16], P('tp'), may hold values from 1 to 5
- w_output: bfloat16 [1024, 2048], P('tp'), may hold values from -0.75 to 0.75
- tokens_second: bfloat16 [1024, 2048], P('ep'), may hold values from -6 to 6
- ffn_gain: float32 [2048], replicated, may hold values from 0.1 to 1.9
- routes: int32 [1024, 4], P('ep'), may hold values from 0 to 15, all different within a row; in each aligned block of 128 rows (0 to 127, 128 to 255, ...) at most 64 rows name the same one
- route_weight: float32 [1024, 4], P('ep'), may hold values from 0.2 to 1.5
- w_gate_exp: bfloat16 [16, 2048, 2048], P('ep', None, 'tp'), may hold values from -0.125 to 0.125
- w_up_exp: bfloat16 [16, 2048, 2048], P('ep', None, 'tp'), may hold values from -0.125 to 0.125
- w_down_exp: bfloat16 [16, 2048, 2048], P('ep', 'tp'), may hold values from -0.125 to 0.125
- w_gate_shared: bfloat16 [2048, 1024], P(None, 'tp'), may hold values from -0.125 to 0.125
- w_up_shared: bfloat16 [2048, 1024], P(None, 'tp'), may hold values from -0.125 to 0.125
- w_down_shared: bfloat16 [1024, 2048], P('tp'), may hold values from -0.1875 to 0.1875
Outputs:
- mixer_out: bfloat16 [4096, 2048], P(('ep', 'tp'))
- moe_out: bfloat16 [1024, 2048], P('ep', 'tp')
Inputs may be any that keep to these rules, and one draw needn't show every extreme that they name: `routes`: each row names 4 different experts; among the rows of one index of ep no expert is named more than 64 times, a bound that some block reaches.
All inputs are finite; a program needn't handle non-finite values.
Results may differ from a plain program's by a relative error of at most 0.017.
Values may be sent and summed in bfloat16 or wider, within the bound.
No kernel may reach another device: no remote copies, remote signals or barrier semaphores. Data moves between devices by JAX's collectives and lax.ppermute only.
A program may use at most 64 MiB of HBM per device.

v0:
```python
import jax
import jax.numpy as jnp
from jax import lax
from jax.sharding import PartitionSpec as P

MODEL_WIDTH = 2048
HEAD_SIZE = 64
BAND_LENGTH = 128


rope_base = 10000.0
norm_eps = 1e-06


def from_behind(value, axis, by):
    devices = lax.axis_size(axis)
    pairs = [(i, i + by) for i in range(devices) if 0 <= i + by < devices]
    return lax.ppermute(value, axis, pairs)


def rms_scale(inputs, gain):
    wide = inputs.astype(jnp.float32)
    scaled = wide * lax.rsqrt(jnp.mean(wide * wide, axis=-1, keepdims=True) + norm_eps)
    return (scaled * gain).astype(jnp.bfloat16)


def apply_rotary(heads, token_positions):
    freqs = rope_base ** (-jnp.arange(0, HEAD_SIZE, 2, dtype=jnp.float32) / HEAD_SIZE)
    angles = token_positions[:, None] * freqs[None, :]
    cosine = jnp.cos(angles)[:, None, :]
    sine = jnp.sin(angles)[:, None, :]
    first_half, second_half = jnp.split(heads, 2, axis=-1)
    return jnp.concatenate(
        [first_half * cosine - second_half * sine, second_half * cosine + first_half * sine],
        axis=-1,
    )


def local(
    tokens_first,
    attn_gain,
    w_query,
    key_matrix,
    value_matrix,
    head_sink_logit,
    w_output,
    tokens_second,
    ffn_gain,
    routes,
    route_weight,
    w_gate_exp,
    w_up_exp,
    w_down_exp,
    w_gate_shared,
    w_up_shared,
    w_down_shared,
):
    rows_first = tokens_first.shape[0]
    norm_input = rms_scale(tokens_first, attn_gain)
    offset = lax.axis_index("ep") * rows_first
    token_positions = (offset + jnp.arange(rows_first, dtype=jnp.int32)).astype(jnp.float32)
    head_count = w_query.shape[1] // HEAD_SIZE
    key_heads = key_matrix.shape[1] // HEAD_SIZE
    head_group = head_count // key_heads
    query_rows = apply_rotary(
        jnp.dot(norm_input, w_query, preferred_element_type=jnp.float32).reshape(
            rows_first, head_count, HEAD_SIZE
        ),
        token_positions,
    ).astype(jnp.bfloat16)
    keys_local = apply_rotary(
        jnp.dot(norm_input, key_matrix, preferred_element_type=jnp.float32).reshape(
            rows_first, key_heads, HEAD_SIZE
        ),
        token_positions,
    ).astype(jnp.bfloat16)
    values_local = (
        jnp.dot(norm_input, value_matrix, preferred_element_type=jnp.float32)
        .astype(jnp.bfloat16)
        .reshape(rows_first, key_heads, HEAD_SIZE)
    )
    keys_before, values_before = from_behind(
        (keys_local[rows_first - BAND_LENGTH :], values_local[rows_first - BAND_LENGTH :]), "ep", 1
    )
    keys_all = jnp.concatenate([keys_before, keys_local], axis=0)
    values_all = jnp.concatenate([values_before, values_local], axis=0)
    layer_block = min(512, rows_first)
    sink_scores = head_sink_logit.reshape(key_heads, head_group)[:, :, None, None]

    def attend(index):
        leading_row = index * layer_block
        block_queries = query_rows.reshape(layer_block, key_heads, head_group, HEAD_SIZE)
        scores = jnp.einsum(
            "qhgd,khd->hgqk", block_queries, keys_all, preferred_element_type=jnp.float32
        ) * HEAD_SIZE ** (-0.5)
        query_pos = offset + leading_row + jnp.arange(layer_block, dtype=jnp.int32)
        key_pos = (
            offset
            + leading_row
            - BAND_LENGTH
            + jnp.arange(layer_block + BAND_LENGTH, dtype=jnp.int32)
        )
        offsets = query_pos[:, None] - key_pos[None, :]
        visible = (offsets >= 0) & (offsets < BAND_LENGTH) & (key_pos[None, :] >= 0)
        scores = jnp.where(visible[None, None], scores, -jnp.inf)
        peak = jnp.maximum(jnp.max(scores, axis=-1, keepdims=True), sink_scores)
        expo = jnp.exp(scores - peak)
        total = jnp.sum(expo, axis=-1, keepdims=True) + jnp.exp(sink_scores - peak)
        weights = (expo / total).astype(jnp.bfloat16)
        mixed = jnp.einsum(
            "hgqk,khd->qhgd", weights, values_all, preferred_element_type=jnp.float32
        )
        return mixed.astype(jnp.bfloat16).reshape(layer_block, head_count * HEAD_SIZE)

    attended = lax.map(attend, jnp.arange(rows_first // layer_block, dtype=jnp.int32)).reshape(
        rows_first, head_count * HEAD_SIZE
    )
    mixer_out = lax.psum_scatter(
        jnp.dot(attended, w_output, preferred_element_type=jnp.float32).astype(jnp.bfloat16),
        "tp",
        scatter_dimension=0,
        tiled=True,
    )
    rows_second = tokens_second.shape[0]
    topk = routes.shape[1]
    exp_dev = w_gate_exp.shape[0]
    n_expdev = lax.axis_size("ep")
    experts = exp_dev * n_expdev
    capacity = max(2, 2 * rows_second * topk // experts)
    slot_count = experts * capacity
    normed_second = rms_scale(tokens_second, ffn_gain)
    flat = routes.reshape(-1)
    onehot = (flat[:, None] == jnp.arange(experts, dtype=jnp.int32)[None, :]).astype(jnp.int32)
    ranks = jnp.sum((jnp.cumsum(onehot, axis=0) - onehot) * onehot, axis=1)
    slots = flat * capacity + ranks
    match = (jnp.arange(slot_count, dtype=jnp.int32)[:, None] == slots[None, :]).reshape(
        slot_count, rows_second, topk
    )
    dispatch = jnp.sum(match.astype(jnp.float32), axis=2).astype(jnp.bfloat16)
    combine = jnp.sum(match.astype(jnp.float32) * route_weight[None, :, :], axis=2)
    width = normed_second.shape[1] // lax.axis_size("tp")
    feature_slice = lax.dynamic_slice_in_dim(normed_second, lax.axis_index("tp") * width, width, 1)
    outgoing = jnp.dot(dispatch, feature_slice, preferred_element_type=jnp.float32).astype(
        jnp.bfloat16
    )
    arrived = lax.all_to_all(outgoing, "ep", split_axis=0, concat_axis=0, tiled=True)
    piece = lax.all_gather(arrived, "tp", axis=1, tiled=True)
    cols = piece.shape[1]
    part = piece.reshape(n_expdev, exp_dev, capacity, cols)
    gate_pre = jnp.einsum("sjcd,jdf->sjcf", part, w_gate_exp, preferred_element_type=jnp.float32)
    up_pre = jnp.einsum("sjcd,jdf->sjcf", part, w_up_exp, preferred_element_type=jnp.float32)
    hidden = (jax.nn.silu(gate_pre) * up_pre).astype(jnp.bfloat16)
    shared_hidden = (
        jax.nn.silu(jnp.dot(normed_second, w_gate_shared, preferred_element_type=jnp.float32))
        * jnp.dot(normed_second, w_up_shared, preferred_element_type=jnp.float32)
    ).astype(jnp.bfloat16)
    routed_term = jnp.einsum(
        "sjcf,jfd->dsjc", hidden, w_down_exp, preferred_element_type=jnp.float32
    ).reshape(lax.axis_size("tp") * (MODEL_WIDTH // lax.axis_size("tp")), slot_count)
    shared_term = lax.dot_general(
        w_down_shared, shared_hidden, (((0,), (1,)), ((), ())), preferred_element_type=jnp.float32
    )
    summed = lax.psum_scatter(
        jnp.concatenate([routed_term, shared_term], axis=1).astype(jnp.bfloat16),
        "tp",
        scatter_dimension=0,
        tiled=True,
    ).astype(jnp.float32)
    routed_part = summed[:, :slot_count].astype(jnp.bfloat16)
    returned = lax.all_to_all(routed_part, "ep", split_axis=1, concat_axis=1, tiled=True)
    weighted = lax.dot_general(
        combine,
        returned.astype(jnp.float32),
        (((0,), (1,)), ((), ())),
        precision=lax.Precision.HIGHEST,
    )
    moe_out = (weighted + summed[:, slot_count:].T).astype(jnp.bfloat16)
    return (mixer_out, moe_out)


def solution(mesh):
    in_specs = (
        P("ep", None),
        P(),
        P(None, "tp"),
        P(None, "tp"),
        P(None, "tp"),
        P("tp"),
        P("tp", None),
        P("ep", None),
        P(),
        P("ep", None),
        P("ep", None),
        P("ep", None, "tp"),
        P("ep", None, "tp"),
        P("ep", "tp", None),
        P(None, "tp"),
        P(None, "tp"),
        P("tp", None),
    )
    out_specs = (P(("ep", "tp"), None), P("ep", "tp"))
    return jax.shard_map(local, mesh=mesh, in_specs=in_specs, out_specs=out_specs, check_vma=False)
```

profile of v0, /device:TPU:0, one launch (start us, length us, event | category | flops | bytes accessed | tf_op | source)
XLA Modules:
  0.0 194.5 jit_solution(10042323882435477261)
XLA Ops:
  7.2 0.0 copy-start
  7.2 0.0 all-gather.2.cloned.1.call-start
  7.2 0.9 copy.42
  8.2 0.1 eq.40
  8.3 0.1 eq.44
  8.4 1.2 reduce-window.6
  9.5 0.2 slice_reduce_fusion
  9.8 0.1 fusion.58
  9.9 0.1 reduce_sum.60
  10.0 0.1 copy.45
  10.1 0.7 multiply_add_fusion
  10.8 1.2 fusion.34
  12.0 1.2 convert_reduce_fusion
  13.2 1.2 fusion.36
  14.4 0.4 convolution_convert_fusion.2
  14.9 32.9 %all_to_all.24 = bf16[8,128,512]{2,1,0:T(8,128)(2,1)} all-to-all(bf16[8,128,512]{2,1,0:T(8,128)(2,1)S(1)} %bitcast.121), channel_id=1, replica_groups=mesh['ep'=8,'tp'=4] {'ep'}, dimensions={0} | all-to-all | bytes 2097152 | tf_op jit(solution)/shard_map/all_to_all | solution.py:146
  47.8 0.0 all-gather.2.cloned.1.call-update
  47.8 0.0 reduce-scatter.5.cloned.1.call-start
  47.9 0.3 fusion.73
  48.2 2.3 %fusion.16 = bf16[2048,128]{0,1:T(8,128)(2,1)S(1)} fusion(bf16[256,2048]{1,0:T(8,128)(2,1)} %param.33, bf16[128,2048]{1,0:T(8,128)(2,1)S(1)} %fusion.36, bf16[2048,256]{1,0:T(8,128)(2,1)} %param.32, f32[128,256]{1,0:T(8,128)S(1)} %fusion.73), kind=kOutput, calls=%fused_computation.23 | convolution fusion | flops 268894208 | bytes 3276800 | tf_op jit(solution)/shard_map/dot_general | solution.py:160
  50.5 30.9 %all-gather.2.cloned.1.call-done = bf16[1024,2048]{1,0:T(8,128)(2,1)} async-done(((bf16[1024,512]{1,0:T(8,128)(2,1)}), bf16[1024,2048]{1,0:T(8,128)(2,1)}) %all-gather.2.cloned.1.call-update) | async-done | bytes 4194320 | tf_op jit(solution)/shard_map/all_gather | solution.py:147
  81.5 7.2 %fusion.8 = f32[2,8,64,512]{3,2,1,0:T(8,128)} fusion(bf16[2,2048,512]{2,1,0:T(8,128)(2,1)} %param.28, bf16[8,2,64,2048]{3,2,1,0:T(8,128)(2,1)} %bitcast.130), kind=kOutput, calls=%fused_computation.14 | convolution fusion | flops 2147483648 | bytes 10485760 | tf_op jit(solution)/shard_map/sjcd,jdf->sjcf/dot_general | solution.py:150
  88.7 11.8 %convert_bitcast_fusion = bf16[2048,8,2,64]{0,3,1,2:T(8,128)(2,1)} fusion(bf16[2,512,2048]{2,1,0:T(8,128)(2,1)} %param.30, f32[2,8,64,512]{3,2,1,0:T(8,128)} %fusion.8, bf16[2,2048,512]{2,1,0:T(8,128)(2,1)} %param.29, bf16[8,2,64,2048]{3,2,1,0:T(8,128)(2,1)} %bitcast.131), kind=kOutput, calls=%fused_computation.16 | convolution fusion | flops 4300210176 | bytes 18874368 | tf_op jit(solution)/shard_map/sjcf,jfd->dsjc/dot_general | solution.py:157
  100.5 2.5 %copy.48 = bf16[2048,8,2,64]{0,3,2,1:T(8,128)(2,1)S(1)} copy(bf16[2048,8,2,64]{0,3,1,2:T(8,128)(2,1)} %convert_bitcast_fusion) | data formatting | bytes 8388608 | tf_op jit(solution)/shard_map/sjcf,jfd->dsjc/transpose | solution.py:157
  103.0 2.5 %pad_maximum_fusion = bf16[2048,1152]{0,1:T(8,128)(2,1)} fusion(bf16[2048,128]{0,1:T(8,128)(2,1)S(1)} %fusion.16, bf16[2048,1024]{0,1:T(8,128)(2,1)S(1)} %bitcast.118), kind=kLoop, calls=%fused_computation.5 | loop fusion | flops 9437184 | bytes 9437184 | tf_op jit(solution)/shard_map/concatenate | solution.py:164
  105.5 0.0 reduce-scatter.5.cloned.1.call-update
  105.5 0.0 reduce-scatter.3.cloned.1.call-start
  105.6 2.2 %fusion.1 = f32[512]{0:T(512)S(1)} fusion(bf16[512,2048]{1,0:T(8,128)(2,1)} %param.17), kind=kLoop, calls=%fused_computation.7 | loop fusion | flops 3145216 | bytes 2099200 | tf_op jit(solution)/shard_map/reduce_sum | solution.py:23
  107.9 0.3 multiply_cosine_fusion
  108.2 2.6 %fusion.70 = f32[512,128]{0,1:T(8,128)S(1)} fusion(bf16[2048,128]{1,0:T(8,128)(2,1)S(1)} %copy-done.4, bf16[512,2048]{1,0:T(8,128)(2,1)} %param.17, f32[2048]{0:T(1024)S(1)} %copy-done.5, f32[512]{0:T(512)S(1)} %add_rsqrt_fusion), kind=kOutput, calls=%fused_computation.105 | convolution fusion | flops 272629760 | bytes 2893824 | tf_op jit(solution)/shard_map/dot_general | solution.py:72
  110.9 4.0 %collective-permute-start.1 = (bf16[128,2,64]{0,2,1:T(8,128)(2,1)S(1)}, bf16[128,2,64]{0,2,1:T(8,128)(2,1)}, u32[]{:S(2)}, u32[]{:S(2)}) collective-permute-start(bf16[128,2,64]{0,2,1:T(8,128)(2,1)S(1)} %pad_maximum_fusion.1), channel_id=1, source_target_pairs={{0,4},{4,8},{8,12},{12,16},{16,20},{20,24},{24,28},{1,5},{5,9},{9,... | collective-permute-start | bytes 98312 | tf_op jit(solution)/shard_map/ppermute | solution.py:18
  114.8 2.1 %convolution_convert_fusion.3 = bf16[512,128]{0,1:T(8,128)(2,1)S(1)} fusion(bf16[2048,128]{1,0:T(8,128)(2,1)} %param.21, bf16[512,2048]{1,0:T(8,128)(2,1)S(1)} %copy-done.1, f32[2048]{0:T(1024)S(1)} %copy-done.5, f32[512]{0:T(512)S(1)} %add_rsqrt_fusion), kind=kOutput, calls=%fused_computation.43 | convolution fusion | flops 272695296 | bytes 2762752 | tf_op jit(solution)/shard_map/dot_general | solution.py:78
  116.9 3.6 %collective-permute-start = (bf16[128,2,64]{0,2,1:T(8,128)(2,1)S(1)}, bf16[128,2,64]{0,2,1:T(8,128)(2,1)}, u32[]{:S(2)}, u32[]{:S(2)}) collective-permute-start(bf16[128,2,64]{0,2,1:T(8,128)(2,1)S(1)} %bitcast.128), channel_id=1, source_target_pairs={{0,4},{4,8},{8,12},{12,16},{16,20},{20,24},{24,28},{1,5},{5,9},{9,... | collective-permute-start | bytes 98312 | tf_op jit(solution)/shard_map/ppermute | solution.py:18
  120.5 2.5 %fusion.68 = f32[512,256]{0,1:T(8,128)S(1)} fusion(bf16[2048,256]{1,0:T(8,128)(2,1)S(1)} %copy-done.3, bf16[512,2048]{1,0:T(8,128)(2,1)} %param.17, f32[2048]{0:T(1024)S(1)} %copy-done.5, f32[512]{0:T(512)S(1)} %add_rsqrt_fusion), kind=kOutput, calls=%fused_computation.104 | convolution fusion | flops 541065216 | bytes 3680256 | tf_op jit(solution)/shard_map/dot_general | solution.py:66
  123.0 0.1 subtract_convert_fusion
  123.1 0.4 fusion.30
  123.6 0.1 max.22
  123.6 1.8 fusion.10
  125.5 0.1 broadcast_maximum_fusion
  125.6 1.1 fusion
  126.7 0.1 exponential_add_fusion
  126.8 2.4 %fusion.31 = bf16[2,64,2,512]{3,1,2,0:T(8,128)(2,1)S(1)} fusion(f32[2,640,512,2]{2,1,3,0:T(8,128)S(1)} %get-tuple-element.32, f32[2,2,512]{2,1,0:T(2,128)S(1)} %exponential_add_fusion, f32[2,2,512]{2,1,0:T(2,128)S(1)} %broadcast_maximum_fusion, pred[512,640]{0,1:T(8,128)(4,1)S(1)} %fusion.30, bf16[512,2,64]{0,2,1:T(8,128)(2,1)S(1)} %bitcast.129, ...), kind=kOutput, calls=%fused_computation.41 | convolution fusion | flops 174784512 | bytes 6012928 | tf_op jit(solution)/shard_map/while/body/eval_jaxpr/hgqk,khd->qhgd/dot_general | solution.py:110
  129.2 2.1 %convolution_convert_fusion = bf16[512,2048]{1,0:T(8,128)(2,1)} fusion(bf16[512,256]{0,1:T(8,128)(2,1)S(1)} %bitcast.123, bf16[256,2048]{1,0:T(8,128)(2,1)S(1)} %copy-done), kind=kOutput, calls=%fused_computation.20 | convolution fusion | flops 537919488 | bytes 3407872 | tf_op jit(solution)/shard_map/dot_general | solution.py:119
  131.3 0.0 reduce-scatter.3.cloned.1.call-update
  131.4 22.1 %reduce-scatter.5.cloned.1.call-done = bf16[512,1152]{0,1:T(8,128)(2,1)} async-done(((bf16[2048,1152]{0,1:T(8,128)(2,1)}), bf16[512,1152]{0,1:T(8,128)(2,1)}) %reduce-scatter.5.cloned.1.call-update) | async-done | bytes 1179664 | tf_op jit(solution)/shard_map/reduce_scatter | solution.py:163
  153.5 1.3 slice.32
  154.8 30.9 %all_to_all.25 = bf16[512,8,128]{0,2,1:T(8,128)(2,1)S(1)} all-to-all(bf16[512,8,128]{0,2,1:T(8,128)(2,1)S(1)} %bitcast.122), channel_id=1, replica_groups=mesh['ep'=8,'tp'=4] {'ep'}, dimensions={1} | all-to-all | bytes 2097152 | tf_op jit(solution)/shard_map/all_to_all | solution.py:170
  185.7 2.3 %fusion.32 = bf16[128,512]{1,0:T(8,128)(2,1)} fusion(f32[1024,128]{1,0:T(8,128)S(1)} %get-tuple-element.17, bf16[512,1024]{0,1:T(8,128)(2,1)S(1)} %bitcast.119, bf16[512,1152]{0,1:T(8,128)(2,1)} %reduce-scatter.5.cloned.1.call-done), kind=kOutput, calls=%fused_computation.44 | convolution fusion | flops 805502976 | bytes 1835008 | tf_op jit(solution)/shard_map/dot_general | solution.py:171
  (29 shorter events, 0.2 us)
Async XLA Ops:
  7.2 122.1 %copy-start = (bf16[256,2048]{1,0:T(8,128)(2,1)S(1)}, bf16[256,2048]{1,0:T(8,128)(2,1)}, u32[]{:S(2)}) copy-start(bf16[256,2048]{1,0:T(8,128)(2,1)} %param.23) | copy-start | bytes 3145732
  7.2 40.7 %copy-start.2 = (bf16[2048,256]{1,0:T(8,128)(2,1)S(1)}, bf16[2048,256]{1,0:T(8,128)(2,1)}, u32[]{:S(2)}) copy-start(bf16[2048,256]{1,0:T(8,128)(2,1)} %param.31) | copy-start | bytes 3145732
  7.2 74.3 %all-gather.2.cloned.1.call-start = ((), (), s32[]{:S(2)}) async-start(), calls=%async_computation.5 | async-start | bytes 5242880 | tf_op jit(solution)/shard_map/all_gather | solution.py:147
  47.8 105.6 %reduce-scatter.5.cloned.1.call-start = ((), (), s32[]{:S(2)}) async-start(), calls=%async_computation.6 | async-start | bytes 5898240 | tf_op jit(solution)/shard_map/reduce_scatter | solution.py:163
  105.5 2.7 %copy-start.4 = (bf16[2048,128]{1,0:T(8,128)(2,1)S(1)}, bf16[2048,128]{1,0:T(8,128)(2,1)}, u32[]{:S(2)}) copy-start(bf16[2048,128]{1,0:T(8,128)(2,1)} %param.20) | copy-start | bytes 1572868
  105.5 2.7 %copy-start.5 = (f32[2048]{0:T(1024)S(1)}, f32[2048]{0:T(1024)}, u32[]{:S(2)}) copy-start(f32[2048]{0:T(1024)} %param.18) | copy-start | bytes 24580
  105.5 82.5 %reduce-scatter.3.cloned.1.call-start = ((), (), s32[]{:S(2)}) async-start(), calls=%async_computation.4 | async-start | bytes 2621440 | tf_op jit(solution)/shard_map/reduce_scatter | solution.py:118
  105.6 9.3 %copy-start.1 = (bf16[512,2048]{1,0:T(8,128)(2,1)S(1)}, bf16[512,2048]{1,0:T(8,128)(2,1)}, u32[]{:S(2)}) copy-start(bf16[512,2048]{1,0:T(8,128)(2,1)} %param.17) | copy-start | bytes 6291460
  108.2 12.3 %copy-start.3 = (bf16[2048,256]{1,0:T(8,128)(2,1)S(1)}, bf16[2048,256]{1,0:T(8,128)(2,1)}, u32[]{:S(2)}) copy-start(bf16[2048,256]{1,0:T(8,128)(2,1)} %param.19) | copy-start | bytes 3145732
  110.9 12.8 %collective-permute-start.1 = (bf16[128,2,64]{0,2,1:T(8,128)(2,1)S(1)}, bf16[128,2,64]{0,2,1:T(8,128)(2,1)}, u32[]{:S(2)}, u32[]{:S(2)}) collective-permute-start(bf16[128,2,64]{0,2,1:T(8,128)(2,1)S(1)} %pad_maximum_fusion.1), channel_id=1, source_target_pairs={{0,4},{4,8},{8,12},{12,16},{16,20},{20,24},{24,28},{1,5},{5,9},{9,... | collective-permute-start | bytes 98312 | tf_op jit(solution)/shard_map/ppermute | solution.py:18
  116.9 6.7 %copy-start.6 = (f32[4]{0:T(128)S(1)}, f32[4]{0:T(128)}, u32[]{:S(2)}) copy-start(f32[4]{0:T(128)} %param.22) | copy-start | bytes 52
  116.9 9.9 %collective-permute-start = (bf16[128,2,64]{0,2,1:T(8,128)(2,1)S(1)}, bf16[128,2,64]{0,2,1:T(8,128)(2,1)}, u32[]{:S(2)}, u32[]{:S(2)}) collective-permute-start(bf16[128,2,64]{0,2,1:T(8,128)(2,1)S(1)} %bitcast.128), channel_id=1, source_target_pairs={{0,4},{4,8},{8,12},{12,16},{16,20},{20,24},{24,28},{1,5},{5,9},{9,... | collective-permute-start | bytes 98312 | tf_op jit(solution)/shard_map/ppermute | solution.py:18
Sparse Core Ops, SparseCore 0:
  48.0 33.4 all-gather.1
  105.6 47.7 reduce-scatter.4
  156.6 31.1 reduce-scatter.2
where the time goes:
time: 195 us
  blocking collectives  63.9 us (33%)
  waiting for transfers between devices  53.1 us (27%)
  matrix products  37.9 us (19%)
  between operations  14 us (7%)
  other arithmetic  12.5 us (6%)
  starting transfers between devices  7.63 us (4%)
  local copies, waits for them, and re-layouts  5.45 us (3%)
    all_to_all x1, blocking collectives, local(): lax.all_to_all(outgoing, 'ep', split_axis=0, concat_axis=0, tiled=True)  32.9 us
    all_gather x1, waiting for transfers between devices, local(): piece = lax.all_gather(arrived, 'tp', axis=1, tiled=True)  30.9 us
    all_to_all x1, blocking collectives, local(): lax.all_to_all(routed_part, 'ep', split_axis=1, concat_axis=1, tiled=True)  30.9 us
    reduce_scatter x1, waiting for transfers between devices, local(): lax.psum_scatter(jnp.concatenate([routed_term, shared_term], axis=1).asty...  22.1 us
    dot_general x1, matrix products, local(): jnp.einsum('sjcf,jfd->dsjc', hidden, w_down_exp, preferred_element_type=j...  11.8 us
    ppermute x2, starting transfers between devices, from_behind(): return lax.ppermute(value, axis, pairs)  7.51 us
    dot_general x1, matrix products, local(): jnp.einsum('sjcd,jdf->sjcf', part, w_gate_exp, preferred_element_type=jnp...  7.19 us
  transfers between devices with their start and end apart: 5, of which 2 were waited for; matrix products, arithmetic and copies ran while one was open for 12% of the time, Pallas kernels for 0%

commit v1 on v0

v1 whole, which is shorter than its diff:
```python
import functools

import jax
import jax.numpy as jnp
from jax import lax
from jax.experimental import pallas as pl
from jax.experimental.pallas import tpu as pltpu
from jax.sharding import PartitionSpec as P

HEAD_SIZE = 64
BAND_LENGTH = 128


rope_base = 10000.0
norm_eps = 1e-06


LANES = 128
SMEM = pl.BlockSpec(memory_space=pltpu.SMEM)
HBM = pl.BlockSpec(memory_space=pltpu.HBM)
VMEM = pl.BlockSpec(memory_space=pltpu.VMEM)


def swap(value, ep_bits, tp_bits):
    ep, tp = lax.axis_size("ep"), lax.axis_size("tp")
    pairs = [
        (e * tp + t, (e ^ ep_bits) * tp + (t ^ tp_bits)) for e in range(ep) for t in range(tp)
    ]
    return lax.ppermute(value, ("ep", "tp"), pairs)


def limit(mib):
    return pltpu.CompilerParams(vmem_limit_bytes=mib << 20)


def in_hbm(*values):
    return [pltpu.with_memory_space_constraint(value, pltpu.HBM) for value in values]


def load(pairs, sems):
    copies = [pltpu.make_async_copy(a, b, sems.at[i]) for i, (a, b) in enumerate(pairs)]
    for copy in copies:
        copy.start()
    return copies


def turn(values, cosine, sine):
    width = values.shape[1]
    half = HEAD_SIZE // 2
    lane = lax.broadcasted_iota(jnp.int32, values.shape, 1)
    upper = pltpu.roll(values, half, 1)
    lower = pltpu.roll(values, width - half, 1)
    other = jnp.where(lane % HEAD_SIZE < half, -lower, upper)
    repeat = width // LANES
    if repeat > 1:
        cosine = jnp.concatenate([cosine] * repeat, axis=1)
        sine = jnp.concatenate([sine] * repeat, axis=1)
    return values * cosine + other * sine


def project_kernel(*refs):
    sources, (cosine, sine), (queries, pairs, last) = refs[:5], refs[5:7], refs[7:10]
    (tokens, gain, query_w, key_w, value_w), sems = refs[10:15], refs[15]
    rows = tokens.shape[0]
    step = min(128, rows)
    parts = [slice(low, low + step) for low in range(0, rows, step)]
    first = [(sources[1], gain)] + [(sources[0].at[p, :], tokens.at[p, :]) for p in parts[:1]]
    rest = [(sources[i], refs[10 + i]) for i in (2, 3, 4)]
    rest += [(sources[0].at[p, :], tokens.at[p, :]) for p in parts[1:]]
    copies = load(first + rest, sems)
    for number, part in enumerate(parts):
        for copy in copies[:2] if number == 0 else copies[4 + number : 5 + number]:
            copy.wait()
        wide = tokens[part, :].astype(jnp.float32)
        scaled = wide * lax.rsqrt(jnp.mean(wide * wide, axis=-1, keepdims=True) + norm_eps)
        normed = (scaled * gain[...]).astype(jnp.bfloat16)
        if number == 0:
            for copy in copies[2:5]:
                copy.wait()
        query = jnp.dot(normed, query_w[...], preferred_element_type=jnp.float32)
        turned = turn(query, cosine[part, :], sine[part, :])
        queries[part, :] = turned.astype(jnp.bfloat16) * jnp.bfloat16(HEAD_SIZE ** (-0.5))
        key = jnp.dot(normed, key_w[...], preferred_element_type=jnp.float32)
        value = jnp.dot(normed, value_w[...], preferred_element_type=jnp.float32)
        both = jnp.concatenate([key, value], axis=1)
        lane = lax.broadcasted_iota(jnp.int32, both.shape, 1)
        turned = turn(both, cosine[part, :], sine[part, :])
        pairs[part, :] = jnp.where(lane < key.shape[1], turned, both).astype(jnp.bfloat16)
    last[...] = pairs[rows - BAND_LENGTH :, :]


def attend_kernel(
    meta, sinks, queries, pairs, before, source, send, keep, attended, output_w, sems
):
    (copy,) = load([(source, output_w)], sems)
    rows, q_width = queries.shape
    width = pairs.shape[1] // 2
    groups = q_width // width
    band = BAND_LENGTH
    place = lax.broadcasted_iota(jnp.int32, (band, 2 * band), 0)
    other = lax.broadcasted_iota(jnp.int32, (band, 2 * band), 1)
    within = (other > place) & (other <= place + band)
    first = within & (other >= jnp.where(meta[2] == 0, band, 0))
    for low in range(0, rows, band):
        visible = first if low == 0 else within
        visible = jnp.concatenate([visible] * groups, axis=0)
        if low == 0:
            window = jnp.concatenate([before[...], pairs[:band, :]], axis=0)
        else:
            window = pairs[low - band : low + band, :]
        out = []
        for h in range(width // HEAD_SIZE):
            keys = window[:, h * HEAD_SIZE : (h + 1) * HEAD_SIZE]
            values = window[:, width + h * HEAD_SIZE : width + (h + 1) * HEAD_SIZE]
            heads = range(h * groups, (h + 1) * groups)
            asked = jnp.concatenate(
                [queries[low : low + band, i * HEAD_SIZE : (i + 1) * HEAD_SIZE] for i in heads], axis=0
            )
            score = lax.dot_general(
                asked, keys, (((1,), (1,)), ((), ())), preferred_element_type=jnp.float32
            )
            score = jnp.where(visible, score, -jnp.inf)
            sink = jnp.concatenate([jnp.full((band, 1), sinks[i], jnp.float32) for i in heads], axis=0)
            peak = jnp.maximum(jnp.max(score, axis=1, keepdims=True), sink)
            expo = jnp.exp(score - peak)
            whole = jnp.sum(expo, axis=1, keepdims=True) + jnp.exp(sink - peak)
            weight = (expo * (1.0 / whole)).astype(jnp.bfloat16)
            mixed = jnp.dot(weight, values, preferred_element_type=jnp.float32)
            out += [mixed[i * band : (i + 1) * band] for i in range(groups)]
        attended[low : low + band, :] = jnp.concatenate(out, axis=1).astype(jnp.bfloat16)
    half, count, _ = send.shape
    copy.wait()
    for k in range(2 * half):
        out, g = (send, 2 * k + 1) if k < half else (keep, 2 * (k - half))
        start = pl.multiple_of((meta[0] ^ g) * count, count)
        out[k % half] = jnp.dot(
            attended[pl.ds(start, count), :], output_w[...], preferred_element_type=jnp.float32
        ).astype(jnp.bfloat16)


def pack_kernel(experts, tp, meta, *refs):
    sources, (whole, half, quarter), held, sems = refs[:4], refs[4:7], refs[7:11], refs[11]
    for copy in load(list(zip(sources, held)), sems):
        copy.wait()
    tokens, gain, routes, weight = held
    rows, width = tokens.shape
    wide = tokens[...].astype(jnp.float32)
    scaled = wide * lax.rsqrt(jnp.mean(wide * wide, axis=-1, keepdims=True) + norm_eps)
    whole[:, :width] = (scaled * gain[...]).astype(jnp.bfloat16)
    pad = whole.shape[1] - width
    line = lax.broadcasted_iota(jnp.int32, (pad, rows), 0)
    named = jnp.where(line < experts, line, line - experts)
    dense = jnp.zeros((pad, rows), jnp.float32)
    for k in range(routes.shape[0]):
        dense = dense + jnp.where(named == routes[k : k + 1, :], weight[k : k + 1, :], 0.0)
    high = dense.astype(jnp.bfloat16).astype(jnp.float32)
    cols = jnp.where(line < experts, high, jnp.where(line < 2 * experts, dense - high, 0.0))
    whole[:, width:] = cols.T.astype(jnp.bfloat16)
    part = rows // 2
    half[...] = whole[pl.ds(pl.multiple_of((meta[0] % 2) * part, part), part), :]
    part = rows // tp
    quarter[...] = whole[pl.ds(pl.multiple_of(meta[0] * part, part), part), :]


def pack(meta, tokens, gain, routes, weight, experts):
    rows, width = tokens.shape
    tp = lax.axis_size("tp")
    total = width + -(-2 * experts // LANES) * LANES
    return pl.pallas_call(
        functools.partial(pack_kernel, experts, tp),
        out_shape=tuple(
            jax.ShapeDtypeStruct((n, total), jnp.bfloat16) for n in (rows, rows // 2, rows // tp)
        ),
        in_specs=[SMEM] + [HBM] * 4,
        out_specs=(VMEM,) * 3,
        scratch_shapes=[
            pltpu.VMEM((rows, width), jnp.bfloat16),
            pltpu.VMEM((1, width), jnp.float32),
            pltpu.VMEM(routes.shape[::-1], jnp.int32),
            pltpu.VMEM(weight.shape[::-1], jnp.float32),
            pltpu.SemaphoreType.DMA((4,)),
        ],
        cost_estimate=pl.CostEstimate(flops=1 << 26, bytes_accessed=1 << 20, transcendentals=0),
        compiler_params=limit(8),
        name="pack",
    )(meta, *in_hbm(tokens, gain.reshape(1, -1), routes.T, weight.T))


def join_kernel(*refs):
    for i, ref in enumerate(refs[:-1]):
        refs[-1][i] = ref[...]


def join(parts):
    return pl.pallas_call(
        join_kernel,
        out_shape=jax.ShapeDtypeStruct((len(parts), *parts[0].shape), parts[0].dtype),
        in_specs=[VMEM] * len(parts),
        out_specs=VMEM,
        cost_estimate=pl.CostEstimate(flops=1 << 20, bytes_accessed=1 << 20, transcendentals=0),
        compiler_params=limit(8),
        name="join",
    )(*parts)


def silu(v):
    return v / (1.0 + jnp.exp(-v))


def expert_kernel(places, blocks, experts, shared, meta, *refs):
    pieces, refs = refs[: len(places)], refs[len(places) :]
    weights, refs = refs[: 6 if shared else 3], refs[6 if shared else 3 :]
    send, keep, held, hidden = refs[:4]
    stored, sems = refs[4:-1], refs[-1]
    gate, up, down = stored[:3]
    exp_dev, width, units = gate.shape
    half, rows, slim = send.shape
    size = rows // blocks
    chunk = min(256, units)
    order = [(2 * k + 1 if k < half else 2 * (k - half)) for k in range(2 * half)]
    starts = [pl.multiple_of((meta[0] ^ g) * slim, slim) for g in order]
    copies = {}

    def fetch(key, number, part):
        copies[key] = pltpu.make_async_copy(
            weights[number].at[part], stored[number].at[part], sems.at[len(copies)]
        )
        copies[key].start()

    whole = (slice(None), slice(None))
    for j in range(exp_dev):
        for c in range(0, units, chunk):
            for number in (0, 1):
                fetch((number, j, c), number, (j, slice(None), slice(c, c + chunk)))
    if shared:
        fetch("gate", 3, whole)
        fetch("up", 4, whole)
        fetch("down", 5, whole)
    for k in range(2 * half):
        fetch((2, k), 2, (slice(None), pl.ds(starts[k], slim)))

    for piece, (first, xor, number) in zip(pieces, places):
        part = piece.shape[1]
        where = 0 if xor is None else (meta[0] % number) ^ xor
        for b in range(piece.shape[0]):
            start = pl.multiple_of((first + b) * size + where * part, part)
            held[pl.ds(start, part), :] = piece[b]
    several = max(n for n in (1, 2, 3) if blocks % n == 0)
    most = several * size

    def over_rows(body):
        if most == rows:
            body(pl.ds(0, rows))
        else:

            @pl.loop(0, rows // most)
            def _(i):
                body(pl.ds(pl.multiple_of(i * most, most), most))

    def scale(at, j):
        cols = held[at, width:].astype(jnp.float32)
        lane = lax.broadcasted_iota(jnp.int32, cols.shape, 1)
        mine = meta[1] + j
        chosen = (lane == mine) | (lane == mine + experts)
        return jnp.sum(jnp.where(chosen, cols, 0.0), axis=1, keepdims=True)

    for j in range(exp_dev):
        for c in range(0, units, chunk):
            copies[0, j, c].wait()
            copies[1, j, c].wait()

            def opening(at, j=j, c=c):
                tokens = held[at, :width]
                opened = jnp.dot(tokens, gate[j, :, c : c + chunk], preferred_element_type=jnp.float32)
                lifted = jnp.dot(tokens, up[j, :, c : c + chunk], preferred_element_type=jnp.float32)
                hidden[at, j * units + c : j * units + c + chunk] = (
                    silu(opened) * lifted * scale(at, j)
                ).astype(jnp.bfloat16)

            over_rows(opening)
    if shared:
        copies["gate"].wait()
        copies["up"].wait()
        own = held[:size, :width]
        hidden_sh = (
            silu(jnp.dot(own, stored[3][...], preferred_element_type=jnp.float32))
            * jnp.dot(own, stored[4][...], preferred_element_type=jnp.float32)
        ).astype(jnp.bfloat16)
        copies["down"].wait()
    for k in range(2 * half):
        out = send if k < half else keep
        copies[2, k].wait()

        def closing(at, k=k, out=out):
            result = jnp.dot(
                hidden[at, :], down[:, pl.ds(starts[k], slim)], preferred_element_type=jnp.float32
            )
            if shared:
                extra = jnp.dot(
                    hidden_sh, stored[5][:, pl.ds(starts[k], slim)], preferred_element_type=jnp.float32
                )
                out[k % half, :size, :] = (result[:size] + extra).astype(jnp.bfloat16)
                out[k % half, size:, :] = result[size:].astype(jnp.bfloat16)
            else:
                out[k % half, at, :] = result.astype(jnp.bfloat16)

        over_rows(closing)


def experts_call(meta, pieces, places, blocks, size, gate, up, down, shared, experts):
    exp_dev, width, units = gate.shape
    tp = lax.axis_size("tp")
    rows = blocks * size
    total = pieces[0].shape[-1]
    weights = [gate, up, down.reshape(exp_dev * units, width), *shared]
    out = jax.ShapeDtypeStruct((tp // 2, rows, width // tp), jnp.bfloat16)
    copies = 2 * exp_dev * (units // min(256, units)) + tp + len(shared)
    return pl.pallas_call(
        functools.partial(expert_kernel, tuple(places), blocks, experts, bool(shared)),
        in_specs=[SMEM] + [VMEM] * len(pieces) + [HBM] * len(weights),
        out_specs=(VMEM, VMEM),
        scratch_shapes=[
            pltpu.VMEM((rows, total), jnp.bfloat16),
            pltpu.VMEM((rows, exp_dev * units), jnp.bfloat16),
            *[pltpu.VMEM(w.shape, w.dtype) for w in weights],
            pltpu.SemaphoreType.DMA((copies,)),
        ],
        out_shape=(out, out),
        cost_estimate=pl.CostEstimate(
            flops=6 * rows * width * units * exp_dev,
            bytes_accessed=6 * width * units * exp_dev,
            transcendentals=rows * units * exp_dev,
        ),
        compiler_params=limit(36),
    )(meta, *pieces, *in_hbm(*weights))


def add_up(*parts):
    total = parts[0].astype(jnp.float32)
    for part in parts[1:]:
        total = total + part.astype(jnp.float32)
    return total.astype(jnp.bfloat16)


def local(
    tokens_first,
    attn_gain,
    w_query,
    key_matrix,
    value_matrix,
    head_sink_logit,
    w_output,
    tokens_second,
    ffn_gain,
    routes,
    route_weight,
    w_gate_exp,
    w_up_exp,
    w_down_exp,
    w_gate_shared,
    w_up_shared,
    w_down_shared,
):
    ep, tp = lax.axis_size("ep"), lax.axis_size("tp")
    index = lax.axis_index("tp").astype(jnp.int32)
    exp_dev = w_gate_exp.shape[0]
    experts = exp_dev * ep
    turn_ep = lax.axis_index("ep").astype(jnp.int32)
    meta = jnp.stack([index, turn_ep * exp_dev, turn_ep])
    columns, lines = ep // 2, tp // 2
    rows_second = tokens_second.shape[0]
    whole, half, quarter = pack(meta, tokens_second, ffn_gain, routes, route_weight, experts)
    beside = swap(half, 1, 0)[None]
    around = [swap(quarter, s << 1, 0) for s in range(1, columns)]

    rows_first = tokens_first.shape[0]
    offset = lax.axis_index("ep") * rows_first
    token_positions = (offset + jnp.arange(rows_first, dtype=jnp.int32)).astype(jnp.float32)
    freqs = rope_base ** (-jnp.arange(0, HEAD_SIZE, 2, dtype=jnp.float32) / HEAD_SIZE)
    angles = token_positions[:, None] * jnp.tile(freqs, 2 * LANES // HEAD_SIZE)[None, :]
    wide_kv = key_matrix.shape[1] + value_matrix.shape[1]
    queries, pairs, last = pl.pallas_call(
        project_kernel,
        out_shape=(
            jax.ShapeDtypeStruct((rows_first, w_query.shape[1]), jnp.bfloat16),
            jax.ShapeDtypeStruct((rows_first, wide_kv), jnp.bfloat16),
            jax.ShapeDtypeStruct((BAND_LENGTH, wide_kv), jnp.bfloat16),
        ),
        in_specs=[HBM] * 5 + [VMEM] * 2,
        out_specs=(VMEM,) * 3,
        scratch_shapes=[
            pltpu.VMEM(tokens_first.shape, jnp.bfloat16),
            pltpu.VMEM((1, attn_gain.shape[0]), jnp.float32),
            pltpu.VMEM(w_query.shape, jnp.bfloat16),
            pltpu.VMEM(key_matrix.shape, jnp.bfloat16),
            pltpu.VMEM(value_matrix.shape, jnp.bfloat16),
            pltpu.SemaphoreType.DMA((4 + rows_first // min(128, rows_first),)),
        ],
        cost_estimate=pl.CostEstimate(flops=1 << 30, bytes_accessed=1 << 22, transcendentals=0),
        compiler_params=limit(24),
        name="project",
    )(
        *in_hbm(tokens_first, attn_gain.reshape(1, -1), w_query, key_matrix, value_matrix),
        jnp.cos(angles), jnp.sin(angles),
    )
    before = lax.ppermute(last, "ep", [(i, i + 1) for i in range(ep - 1)])
    count = rows_first // tp
    part = jax.ShapeDtypeStruct((lines, count, w_output.shape[1]), jnp.bfloat16)
    outward, kept = pl.pallas_call(
        attend_kernel,
        out_shape=(part, part),
        in_specs=[SMEM] * 2 + [VMEM] * 3 + [HBM],
        out_specs=(VMEM,) * 2,
        scratch_shapes=[
            pltpu.VMEM((rows_first, w_query.shape[1]), jnp.bfloat16),
            pltpu.VMEM(w_output.shape, jnp.bfloat16),
            pltpu.SemaphoreType.DMA((1,)),
        ],
        cost_estimate=pl.CostEstimate(flops=1 << 30, bytes_accessed=1 << 22, transcendentals=0),
        compiler_params=limit(24),
        name="attend",
    )(meta, head_sink_logit, queries, pairs, before, *in_hbm(w_output))
    outward = swap(outward, 0, 1)
    mixer_out = add_up(
        outward[0],
        kept[0],
        *[swap(add_up(outward[s], kept[s]), 0, s << 1) for s in range(1, lines)],
    )
    along = join(around)
    across = swap(along, 1, 0)
    rest_along, rest_across = [(along, 0)], [(across, 0)]
    for s in range(1, lines):
        other = swap(along, 0, s << 1)
        rest_along.append((other, s << 1))
        rest_across.append((swap(other, 1, 0), s << 1))

    def with_core(listed):
        listed = listed + [(swap(v, 0, 1), x ^ 1) for v, x in listed]
        return [v for v, _ in listed], [(0, x, tp) for _, x in listed]

    near = ([whole[None], beside, swap(beside, 0, 1)], [(0, None, 1), (1, 0, 2), (1, 1, 2)])
    shared = (w_gate_shared, w_up_shared, w_down_shared)
    keep = []
    for name, (pieces, places), blocks, extra in (
        ("near", near, 2, shared),
        ("along", with_core(rest_along), columns - 1, ()),
        ("across", with_core(rest_across), columns - 1, ()),
    ):
        s, k = experts_call(
            meta, pieces, places, blocks, rows_second,
            w_gate_exp, w_up_exp, w_down_exp, extra, experts,
        )
        slim = s.shape[-1]
        sent = swap(s, 0, 1).reshape(lines, blocks, rows_second, slim)
        kept = k.reshape(lines, blocks, rows_second, slim)
        gone = [add_up(sent[i], kept[i]) for i in range(1, lines)]
        if gone and name != "near":
            meta, *gone = lax.optimization_barrier((meta, *gone))
        out = [swap(gone[i - 1], 0, i << 1) for i in range(1, lines)]
        keep.append(add_up(sent[0], kept[0], *out))
    near, along, across = keep
    far = swap(across, 1, 0)
    beside = swap(near[1], 1, 0)
    outgoing = add_up(along, far)
    arrived = [swap(outgoing[s - 1], s << 1, 0) for s in range(1, columns)]
    moe_out = add_up(near[0], beside, *arrived)
    return (mixer_out, moe_out)


def solution(mesh):
    in_specs = (
        P("ep", None),
        P(),
        P(None, "tp"),
        P(None, "tp"),
        P(None, "tp"),
        P("tp"),
        P("tp", None),
        P("ep", None),
        P(),
        P("ep", None),
        P("ep", None),
        P("ep", None, "tp"),
        P("ep", None, "tp"),
        P("ep", "tp", None),
        P(None, "tp"),
        P(None, "tp"),
        P("tp", None),
    )
    out_specs = (P(("ep", "tp"), None), P("ep", "tp"))

    return jax.shard_map(local, mesh=mesh, in_specs=in_specs, out_specs=out_specs, check_vma=False)
```

time: 195 us -> 139 us (0.71)
  blocking collectives: 63.9 us -> 0 us
  Pallas kernels: 0 us -> 39 us
  matrix products: 37.9 us -> 0 us
  starting transfers between devices: 7.63 us -> 26.8 us
  waiting for transfers between devices: 53.1 us -> 66.8 us
  between operations: 14 us -> 0.83 us
  other arithmetic: 12.5 us -> 5.01 us
  local copies, waits for them, and re-layouts: 5.45 us -> 0.14 us
    ppermute x2 -> x26, waiting for transfers between devices: 0.01 us -> 66.8 us  [the longest x25 66.8 us: swap(): return lax.ppermute(value, ('ep', 'tp'), pairs)]
    all_to_all x2 -> x0, blocking collectives: 63.9 us -> none  [the longest x1 32.9 us: local(): lax.all_to_all(outgoing, 'ep', split_axis=0, concat_axis=0, tiled=True)]
    pallas_call x0 -> x7, Pallas kernels: none -> 39 us  [the longest x3 24.6 us: experts_call(): pl.pallas_call(functools.partial(expert_kernel, tuple(places), blocks, ex...]
    dot_general x12 -> x0, matrix products: 37.9 us -> none  [the longest x1 11.8 us: local(): jnp.einsum('sjcf,jfd->dsjc', hidden, w_down_exp, preferred_element_type=j...]
    all_gather x1 -> x0, waiting for transfers between devices: 30.9 us -> none  [local(): piece = lax.all_gather(arrived, 'tp', axis=1, tiled=True)]
    reduce_scatter x2 -> x0, waiting for transfers between devices: 22.1 us -> none  [the longest x1 22.1 us: local(): lax.psum_scatter(jnp.concatenate([routed_term, shared_term], axis=1).asty...]
    ppermute x2 -> x26, starting transfers between devices: 7.51 us -> 26.8 us  [the longest x25 23.2 us: swap(): return lax.ppermute(value, ('ep', 'tp'), pairs)]
    reduce_sum x5 -> x0, other arithmetic: 5.85 us -> none  [the longest x2 3.45 us: rms_scale(): jnp.mean(wide * wide, axis=-1, keepdims=True) + norm_eps]
  transfers between devices with their start and end apart: 5 -> 26, of which waited for: 2 -> 11; matrix products, arithmetic and copies ran while one was open for 12% -> 3% of each run, Pallas kernels for 0% -> 27%
where the time goes in v1:
time: 139 us
  waiting for transfers between devices  66.8 us (48%)
  Pallas kernels  39 us (28%)
  starting transfers between devices  26.8 us (19%)
  other arithmetic  5.01 us (4%)
    ppermute x25, waiting for transfers between devices, swap(): return lax.ppermute(value, ('ep', 'tp'), pairs)  66.8 us
    pallas_call x3, Pallas kernels, experts_call(): pl.pallas_call(functools.partial(expert_kernel, tuple(places), blocks, ex...  24.6 us
    ppermute x25, starting transfers between devices, swap(): return lax.ppermute(value, ('ep', 'tp'), pairs)  23.2 us
    pallas_call x1, Pallas kernels, local(): pl.pallas_call(attend_kernel, out_shape=(part, part), in_specs=[SMEM] * 2...  7.68 us
    pallas_call x1, Pallas kernels, local(): pl.pallas_call(project_kernel, out_shape=(jax.ShapeDtypeStruct((rows_firs...  4.81 us
    ppermute x1, starting transfers between devices, local(): before = lax.ppermute(last, 'ep', [(i, i + 1) for i in range(ep - 1)])  3.58 us
  transfers between devices with their start and end apart: 26, of which 11 were waited for; matrix products, arithmetic and copies ran while one was open for 3% of the time, Pallas kernels for 27%

profile of v1, /device:TPU:0, one launch (start us, length us, event | category | flops | bytes accessed | tf_op | source)
XLA Modules:
  0.0 138.6 jit_solution(8019217119874904126)
XLA Ops:
  0.6 0.1 pad_add_fusion.meta
  0.7 1.9 %pack.1 = (bf16[128,2176]{1,0:T(8,128)(2,1)S(1)}, bf16[64,2176]{1,0:T(8,128)(2,1)S(1)}, bf16[32,2176]{1,0:T(8,128)(2,1)S(1)}) custom-call(s32[3]{0:T(128)S(1)} %pad_add_fusion.meta, bf16[128,2048]{1,0:T(8,128)(2,1)} %refs_0_.3, f32[1,2048]{1,0:T(1,128)} %bitcast.47, s32[4,128]{1,0:T(4,128)} %bitcast.49, f32[4,128]{1,0:T(4,128)} %bitcast.50), custom_call_target="tpu_custom_call" | custom-call | flops 67108864 | bytes 1048576 | tf_op jit(solution)/shard_map/pack/pallas_call | solution.py:169
  2.6 5.1 %collective-permute-start.10 = (bf16[32,2176]{1,0:T(8,128)(2,1)S(1)}, bf16[32,2176]{1,0:T(8,128)(2,1)S(1)}, u32[]{:S(2)}, u32[]{:S(2)}) collective-permute-start(bf16[32,2176]{1,0:T(8,128)(2,1)S(1)} %get-tuple-element.28), channel_id=1, source_target_pairs={{0,24},{1,25},{2,26},{3,27},{4,28},{5,29},{6,30},{7,31},{8,16},{9,... | collective-permute-start | bytes 417800 | tf_op jit(solution)/shard_map/ppermute | solution.py:29
  7.7 0.6 collective-permute-start.9
  8.4 3.9 %collective-permute-done.10.refs_2_ = bf16[32,2176]{1,0:T(8,128)(2,1)S(1)} collective-permute-done((bf16[32,2176]{1,0:T(8,128)(2,1)S(1)}, bf16[32,2176]{1,0:T(8,128)(2,1)S(1)}, u32[]{:S(2)}, u32[]{:S(2)}) %collective-permute-start.10) | collective-permute-done | bytes 139296 | tf_op jit(solution)/shard_map/ppermute | solution.py:29
  12.3 3.2 %collective-permute-done.8.refs_0_ = bf16[32,2176]{1,0:T(8,128)(2,1)S(1)} collective-permute-done((bf16[32,2176]{1,0:T(8,128)(2,1)S(1)}, bf16[32,2176]{1,0:T(8,128)(2,1)S(1)}, u32[]{:S(2)}, u32[]{:S(2)}) %collective-permute-start.8) | collective-permute-done | bytes 139296 | tf_op jit(solution)/shard_map/ppermute | solution.py:29
  15.5 4.0 %collective-permute-done.9.refs_1_ = bf16[32,2176]{1,0:T(8,128)(2,1)S(1)} collective-permute-done((bf16[32,2176]{1,0:T(8,128)(2,1)S(1)}, bf16[32,2176]{1,0:T(8,128)(2,1)S(1)}, u32[]{:S(2)}, u32[]{:S(2)}) %collective-permute-start.9) | collective-permute-done | bytes 139296 | tf_op jit(solution)/shard_map/ppermute | solution.py:29
  19.6 1.6 %collective-permute-start.11 = (bf16[3,32,2176]{2,1,0:T(8,128)(2,1)S(1)}, bf16[3,32,2176]{2,1,0:T(8,128)(2,1)S(1)}, u32[]{:S(2)}, u32[]{:S(2)}) collective-permute-start(bf16[3,32,2176]{2,1,0:T(8,128)(2,1)S(1)} %join.1.refs_0_), channel_id=1, source_target_pairs={{0,2},{1,3},{2,0},{3,1},{4,6},{5,7},{6,4},{7,5},{8,10},{9,11},{10,... | collective-permute-start | bytes 1253384 | tf_op jit(solution)/shard_map/ppermute | solution.py:29
  21.1 9.2 %collective-permute-done.11.refs_1_ = bf16[3,32,2176]{2,1,0:T(8,128)(2,1)S(1)} collective-permute-done((bf16[3,32,2176]{2,1,0:T(8,128)(2,1)S(1)}, bf16[3,32,2176]{2,1,0:T(8,128)(2,1)S(1)}, u32[]{:S(2)}, u32[]{:S(2)}) %collective-permute-start.11) | collective-permute-done | bytes 417824 | tf_op jit(solution)/shard_map/ppermute | solution.py:29
  30.3 1.5 %collective-permute-start.3 = (bf16[64,2176]{1,0:T(8,128)(2,1)S(1)}, bf16[64,2176]{1,0:T(8,128)(2,1)S(1)}, u32[]{:S(2)}, u32[]{:S(2)}) collective-permute-start(bf16[64,2176]{1,0:T(8,128)(2,1)S(1)} %get-tuple-element.25), channel_id=1, source_target_pairs={{0,4},{1,5},{2,6},{3,7},{4,0},{5,1},{6,2},{7,3},{8,12},{9,13},{10,... | collective-permute-start | bytes 835592 | tf_op jit(solution)/shard_map/ppermute | solution.py:29
  31.8 0.3 collective-permute-done.13.refs_3_
  32.1 8.5 %shard_map.177 = (bf16[2,384,512]{2,1,0:T(8,128)(2,1)S(1)}, bf16[2,384,512]{2,1,0:T(8,128)(2,1)S(1)}) custom-call(s32[3]{0:T(128)S(1)} %pad_add_fusion.meta, bf16[3,32,2176]{2,1,0:T(8,128)(2,1)S(1)} %join.1.refs_0_, bf16[3,32,2176]{2,1,0:T(8,128)(2,1)S(1)} %collective-permute-done.11.refs_1_, bf16[3,32,2176]{2,1,0:T(8,128)(2,1)S(1)} %collective-permute-done.12.refs_2_, ...), custom_call_target="tpu_custom_call" | custom-call | flops 4831838208 | bytes 12582912 | tf_op jit(solution)/shard_map/pallas_call | solution.py:318
  40.6 0.2 collective-permute-start.14
  40.9 0.1 mul.36
  40.9 1.5 %collective-permute-start.16 = (bf16[3,32,2176]{2,1,0:T(8,128)(2,1)S(1)}, bf16[3,32,2176]{2,1,0:T(8,128)(2,1)S(1)}, u32[]{:S(2)}, u32[]{:S(2)}) collective-permute-start(bf16[3,32,2176]{2,1,0:T(8,128)(2,1)S(1)} %join.1.refs_0_), channel_id=1, source_target_pairs={{0,4},{1,5},{2,6},{3,7},{4,0},{5,1},{6,2},{7,3},{8,12},{9,13},{10,... | collective-permute-start | bytes 1253384 | tf_op jit(solution)/shard_map/ppermute | solution.py:29
  42.4 0.5 collective-permute-start.17
  43.0 1.0 multiply_sine_fusion
  44.0 4.8 %project.1 = (bf16[512,256]{1,0:T(8,128)(2,1)S(1)}, bf16[512,256]{1,0:T(8,128)(2,1)S(1)}, bf16[128,256]{1,0:T(8,128)(2,1)S(1)}) custom-call(bf16[512,2048]{1,0:T(8,128)(2,1)} %refs_0_.2, f32[1,2048]{1,0:T(1,128)} %bitcast.48, bf16[2048,256]{1,0:T(8,128)(2,1)} %refs_2_.1, bf16[2048,128]{1,0:T(8,128)(2,1)} %refs_3_.2, bf16[2048,128]{1,0:T(8,128)(2,1)} %refs_4_.4, ...), custom_call_target="tpu_custom_call" | custom-call | flops 1073741824 | bytes 4194304 | tf_op jit(solution)/shard_map/project/pallas_call | solution.py:382
  48.8 3.6 %collective-permute-start = (bf16[128,256]{1,0:T(8,128)(2,1)S(1)}, bf16[128,256]{1,0:T(8,128)(2,1)S(1)}, u32[]{:S(2)}, u32[]{:S(2)}) collective-permute-start(bf16[128,256]{1,0:T(8,128)(2,1)S(1)} %get-tuple-element.21), channel_id=1, source_target_pairs={{0,4},{4,8},{8,12},{12,16},{16,20},{20,24},{24,28},{1,5},{5,9},{9,... | collective-permute-start | bytes 196616 | tf_op jit(solution)/shard_map/ppermute | solution.py:406
  52.4 1.1 collective-permute-done.16.refs_0_
  53.5 8.4 %collective-permute-done.17.refs_1_ = bf16[3,32,2176]{2,1,0:T(8,128)(2,1)S(1)} collective-permute-done((bf16[3,32,2176]{2,1,0:T(8,128)(2,1)S(1)}, bf16[3,32,2176]{2,1,0:T(8,128)(2,1)S(1)}, u32[]{:S(2)}, u32[]{:S(2)}) %collective-permute-start.17) | collective-permute-done | bytes 417824 | tf_op jit(solution)/shard_map/ppermute | solution.py:29
  61.8 7.5 %shard_map.176 = (bf16[2,256,512]{2,1,0:T(8,128)(2,1)S(1)}, bf16[2,256,512]{2,1,0:T(8,128)(2,1)S(1)}) custom-call(s32[3]{0:T(128)S(1)} %pad_add_fusion.meta, bf16[1,128,2176]{2,1,0:T(8,128)(2,1)S(1)} %bitcast.35, bf16[1,64,2176]{2,1,0:T(8,128)(2,1)S(1)} %bitcast.37, bf16[1,64,2176]{2,1,0:T(8,128)(2,1)S(1)} %collective-permute-done.4.refs_2_, ...), custom_call_target="tpu_custom_call" | custom-call | flops 3221225472 | bytes 12582912 | tf_op jit(solution)/shard_map/pallas_call | solution.py:318
  69.4 0.6 collective-permute-start.5
  70.0 1.3 convert_add_fusion.1
  71.3 8.5 %shard_map.178 = (bf16[2,384,512]{2,1,0:T(8,128)(2,1)S(1)}, bf16[2,384,512]{2,1,0:T(8,128)(2,1)S(1)}) custom-call(s32[3]{0:T(128)S(1)} %pad_add_fusion.meta, bf16[3,32,2176]{2,1,0:T(8,128)(2,1)S(1)} %collective-permute-done.16.refs_0_, bf16[3,32,2176]{2,1,0:T(8,128)(2,1)S(1)} %collective-permute-done.17.refs_1_, ...), custom_call_target="tpu_custom_call" | custom-call | flops 4831838208 | bytes 12582912 | tf_op jit(solution)/shard_map/pallas_call | solution.py:318
  80.0 7.7 %attend.1 = (bf16[2,128,2048]{2,1,0:T(8,128)(2,1)S(1)}, bf16[2,128,2048]{2,1,0:T(8,128)(2,1)S(1)}) custom-call(s32[3]{0:T(128)S(1)} %pad_add_fusion.meta, f32[4]{0:T(128)S(1)} %copy-done, bf16[512,256]{1,0:T(8,128)(2,1)S(1)} %get-tuple-element.19.queries, bf16[512,256]{1,0:T(8,128)(2,1)S(1)} %get-tuple-element.20.pairs, ...), custom_call_target="tpu_custom_call" | custom-call | flops 1073741824 | bytes 4194304 | tf_op jit(solution)/shard_map/attend/pallas_call | solution.py:409
  87.6 0.6 collective-permute-start.1
  88.2 0.1 add_convert_fusion.7
  88.3 1.6 %collective-permute-start.6 = (bf16[2,128,512]{2,1,0:T(8,128)(2,1)S(1)}, bf16[2,128,512]{2,1,0:T(8,128)(2,1)S(1)}, u32[]{:S(2)}, u32[]{:S(2)}) collective-permute-start(bf16[2,128,512]{2,1,0:T(8,128)(2,1)S(1)} %bitcast.46), channel_id=1, source_target_pairs={{0,2},{1,3},{2,0},{3,1},{4,6},{5,7},{6,4},{7,5},{8,10},{9,11},{10,... | collective-permute-start | bytes 786440 | tf_op jit(solution)/shard_map/ppermute | solution.py:29
  89.9 0.2 add_convert_fusion.3
  90.1 0.6 collective-permute-start.21
  90.7 0.1 fusion.1
  90.8 1.6 %collective-permute-start.2 = (bf16[128,2048]{1,0:T(8,128)(2,1)S(1)}, bf16[128,2048]{1,0:T(8,128)(2,1)S(1)}, u32[]{:S(2)}, u32[]{:S(2)}) collective-permute-start(bf16[128,2048]{1,0:T(8,128)(2,1)S(1)} %fusion.1), channel_id=1, source_target_pairs={{0,2},{1,3},{2,0},{3,1},{4,6},{5,7},{6,4},{7,5},{8,10},{9,11},{10,... | collective-permute-start | bytes 1572872 | tf_op jit(solution)/shard_map/ppermute | solution.py:29
  92.4 0.5 collective-permute-start.15
  92.9 13.1 %collective-permute-done.21 = bf16[3,128,512]{2,1,0:T(8,128)(2,1)S(1)} collective-permute-done((bf16[3,128,512]{2,1,0:T(8,128)(2,1)S(1)}, bf16[3,128,512]{2,1,0:T(8,128)(2,1)S(1)}, u32[]{:S(2)}, u32[]{:S(2)}) %collective-permute-start.21) | collective-permute-done | bytes 393248 | tf_op jit(solution)/shard_map/ppermute | solution.py:29
  106.0 0.1 add_convert_fusion.2
  106.1 2.1 %collective-permute-start.22 = (bf16[3,128,512]{2,1,0:T(8,128)(2,1)S(1)}, bf16[3,128,512]{2,1,0:T(8,128)(2,1)S(1)}, u32[]{:S(2)}, u32[]{:S(2)}) collective-permute-start(bf16[3,128,512]{2,1,0:T(8,128)(2,1)S(1)} %add_convert_fusion.2), channel_id=1, source_target_pairs={{0,4},{1,5},{2,6},{3,7},{4,0},{5,1},{6,2},{7,3},{8,12},{9,13},{10,... | collective-permute-start | bytes 1179656 | tf_op jit(solution)/shard_map/ppermute | solution.py:29
  108.3 0.1 add_convert_fusion.6
  108.4 0.1 collective-permute-start.7
  108.5 16.3 %collective-permute-done.15 = bf16[3,128,512]{2,1,0:T(8,128)(2,1)S(1)} collective-permute-done((bf16[3,128,512]{2,1,0:T(8,128)(2,1)S(1)}, bf16[3,128,512]{2,1,0:T(8,128)(2,1)S(1)}, u32[]{:S(2)}, u32[]{:S(2)}) %collective-permute-start.15) | collective-permute-done | bytes 393248 | tf_op jit(solution)/shard_map/ppermute | solution.py:29
  124.7 0.2 add_convert_fusion.1
  125.0 0.1 collective-permute-start.23
  125.1 2.5 %collective-permute-start.24 = (bf16[128,512]{1,0:T(8,128)(2,1)S(1)}, bf16[128,512]{1,0:T(8,128)(2,1)S(1)}, u32[]{:S(2)}, u32[]{:S(2)}) collective-permute-start(bf16[128,512]{1,0:T(8,128)(2,1)S(1)} %get-tuple-element.44), channel_id=1, source_target_pairs={{0,16},{1,17},{2,18},{3,19},{4,20},{5,21},{6,22},{7,23},{8,24},{9,... | collective-permute-start | bytes 393224 | tf_op jit(solution)/shard_map/ppermute | solution.py:29
  127.5 1.9 %collective-permute-start.25 = (bf16[128,512]{1,0:T(8,128)(2,1)S(1)}, bf16[128,512]{1,0:T(8,128)(2,1)S(1)}, u32[]{:S(2)}, u32[]{:S(2)}) collective-permute-start(bf16[128,512]{1,0:T(8,128)(2,1)S(1)} %get-tuple-element.43), channel_id=1, source_target_pairs={{0,24},{1,25},{2,26},{3,27},{4,28},{5,29},{6,30},{7,31},{8,16},{9,... | collective-permute-start | bytes 393224 | tf_op jit(solution)/shard_map/ppermute | solution.py:29
  129.4 1.0 fusion
  130.5 0.9 collective-permute-done.23
  131.4 6.5 %collective-permute-done.24 = bf16[128,512]{1,0:T(8,128)(2,1)S(1)} collective-permute-done((bf16[128,512]{1,0:T(8,128)(2,1)S(1)}, bf16[128,512]{1,0:T(8,128)(2,1)S(1)}, u32[]{:S(2)}, u32[]{:S(2)}) %collective-permute-start.24) | collective-permute-done | bytes 131104 | tf_op jit(solution)/shard_map/ppermute | solution.py:29
  137.9 0.7 fusion.5
  (30 shorter events, 0.2 us)
Async XLA Ops:
  2.6 9.7 %collective-permute-start.10 = (bf16[32,2176]{1,0:T(8,128)(2,1)S(1)}, bf16[32,2176]{1,0:T(8,128)(2,1)S(1)}, u32[]{:S(2)}, u32[]{:S(2)}) collective-permute-start(bf16[32,2176]{1,0:T(8,128)(2,1)S(1)} %get-tuple-element.28), channel_id=1, source_target_pairs={{0,24},{1,25},{2,26},{3,27},{4,28},{5,29},{6,30},{7,31},{8,16},{9,... | collective-permute-start | bytes 417800 | tf_op jit(solution)/shard_map/ppermute | solution.py:29
  7.7 7.8 %collective-permute-start.8 = (bf16[32,2176]{1,0:T(8,128)(2,1)S(1)}, bf16[32,2176]{1,0:T(8,128)(2,1)S(1)}, u32[]{:S(2)}, u32[]{:S(2)}) collective-permute-start(bf16[32,2176]{1,0:T(8,128)(2,1)S(1)} %get-tuple-element.28), channel_id=1, source_target_pairs={{0,8},{1,9},{2,10},{3,11},{4,12},{5,13},{6,14},{7,15},{8,0},{9,1},... | collective-permute-start | bytes 417800 | tf_op jit(solution)/shard_map/ppermute | solution.py:29
  7.7 11.8 %collective-permute-start.9 = (bf16[32,2176]{1,0:T(8,128)(2,1)S(1)}, bf16[32,2176]{1,0:T(8,128)(2,1)S(1)}, u32[]{:S(2)}, u32[]{:S(2)}) collective-permute-start(bf16[32,2176]{1,0:T(8,128)(2,1)S(1)} %get-tuple-element.28), channel_id=1, source_target_pairs={{0,16},{1,17},{2,18},{3,19},{4,20},{5,21},{6,22},{7,23},{8,24},{9,... | collective-permute-start | bytes 417800 | tf_op jit(solution)/shard_map/ppermute | solution.py:29
  19.6 10.8 %collective-permute-start.11 = (bf16[3,32,2176]{2,1,0:T(8,128)(2,1)S(1)}, bf16[3,32,2176]{2,1,0:T(8,128)(2,1)S(1)}, u32[]{:S(2)}, u32[]{:S(2)}) collective-permute-start(bf16[3,32,2176]{2,1,0:T(8,128)(2,1)S(1)} %join.1.refs_0_), channel_id=1, source_target_pairs={{0,2},{1,3},{2,0},{3,1},{4,6},{5,7},{6,4},{7,5},{8,10},{9,11},{10,... | collective-permute-start | bytes 1253384 | tf_op jit(solution)/shard_map/ppermute | solution.py:29
  21.1 10.7 %collective-permute-start.12 = (bf16[3,32,2176]{2,1,0:T(8,128)(2,1)S(1)}, bf16[3,32,2176]{2,1,0:T(8,128)(2,1)S(1)}, u32[]{:S(2)}, u32[]{:S(2)}) collective-permute-start(bf16[3,32,2176]{2,1,0:T(8,128)(2,1)S(1)} %join.1.refs_0_), channel_id=1, source_target_pairs={{0,1},{1,0},{2,3},{3,2},{4,5},{5,4},{6,7},{7,6},{8,9},{9,8},{10,11... | collective-permute-start | bytes 1253384 | tf_op jit(solution)/shard_map/ppermute | solution.py:29
  30.3 1.8 %collective-permute-start.13 = (bf16[3,32,2176]{2,1,0:T(8,128)(2,1)S(1)}, bf16[3,32,2176]{2,1,0:T(8,128)(2,1)S(1)}, u32[]{:S(2)}, u32[]{:S(2)}) collective-permute-start(bf16[3,32,2176]{2,1,0:T(8,128)(2,1)S(1)} %collective-permute-done.11.refs_1_), channel_id=1, source_target_pairs={{0,1},{1,0},{2,3},{3,2},{4,5},{5,4},{6,7},{7,6},{8,9},{9,8},{10,11... | collective-permute-start | bytes 1253384 | tf_op jit(solution)/shard_map/ppermute | solution.py:29
  30.3 12.6 %collective-permute-start.3 = (bf16[64,2176]{1,0:T(8,128)(2,1)S(1)}, bf16[64,2176]{1,0:T(8,128)(2,1)S(1)}, u32[]{:S(2)}, u32[]{:S(2)}) collective-permute-start(bf16[64,2176]{1,0:T(8,128)(2,1)S(1)} %get-tuple-element.25), channel_id=1, source_target_pairs={{0,4},{1,5},{2,6},{3,7},{4,0},{5,1},{6,2},{7,3},{8,12},{9,13},{10,... | collective-permute-start | bytes 835592 | tf_op jit(solution)/shard_map/ppermute | solution.py:29
  40.6 29.3 %collective-permute-start.14 = (bf16[2,384,512]{2,1,0:T(8,128)(2,1)S(1)}, bf16[2,384,512]{2,1,0:T(8,128)(2,1)}, u32[]{:S(2)}, u32[]{:S(2)}) collective-permute-start(bf16[2,384,512]{2,1,0:T(8,128)(2,1)S(1)} %get-tuple-element.29), channel_id=1, source_target_pairs={{0,1},{1,0},{2,3},{3,2},{4,5},{5,4},{6,7},{7,6},{8,9},{9,8},{10,11... | collective-permute-start | bytes 2359304 | tf_op jit(solution)/shard_map/ppermute | solution.py:29
  40.9 12.5 %collective-permute-start.16 = (bf16[3,32,2176]{2,1,0:T(8,128)(2,1)S(1)}, bf16[3,32,2176]{2,1,0:T(8,128)(2,1)S(1)}, u32[]{:S(2)}, u32[]{:S(2)}) collective-permute-start(bf16[3,32,2176]{2,1,0:T(8,128)(2,1)S(1)} %join.1.refs_0_), channel_id=1, source_target_pairs={{0,4},{1,5},{2,6},{3,7},{4,0},{5,1},{6,2},{7,3},{8,12},{9,13},{10,... | collective-permute-start | bytes 1253384 | tf_op jit(solution)/shard_map/ppermute | solution.py:29
  42.4 19.4 %collective-permute-start.17 = (bf16[3,32,2176]{2,1,0:T(8,128)(2,1)S(1)}, bf16[3,32,2176]{2,1,0:T(8,128)(2,1)S(1)}, u32[]{:S(2)}, u32[]{:S(2)}) collective-permute-start(bf16[3,32,2176]{2,1,0:T(8,128)(2,1)S(1)} %collective-permute-done.11.refs_1_), channel_id=1, source_target_pairs={{0,4},{1,5},{2,6},{3,7},{4,0},{5,1},{6,2},{7,3},{8,12},{9,13},{10,... | collective-permute-start | bytes 1253384 | tf_op jit(solution)/shard_map/ppermute | solution.py:29
  43.0 18.8 %collective-permute-start.4 = (bf16[1,64,2176]{2,1,0:T(8,128)(2,1)S(1)}, bf16[1,64,2176]{2,1,0:T(8,128)(2,1)S(1)}, u32[]{:S(2)}, u32[]{:S(2)}) collective-permute-start(bf16[1,64,2176]{2,1,0:T(8,128)(2,1)S(1)} %bitcast.36), channel_id=1, source_target_pairs={{0,1},{1,0},{2,3},{3,2},{4,5},{5,4},{6,7},{7,6},{8,9},{9,8},{10,11... | collective-permute-start | bytes 835592 | tf_op jit(solution)/shard_map/ppermute | solution.py:29
  48.8 31.1 %collective-permute-start = (bf16[128,256]{1,0:T(8,128)(2,1)S(1)}, bf16[128,256]{1,0:T(8,128)(2,1)S(1)}, u32[]{:S(2)}, u32[]{:S(2)}) collective-permute-start(bf16[128,256]{1,0:T(8,128)(2,1)S(1)} %get-tuple-element.21), channel_id=1, source_target_pairs={{0,4},{4,8},{8,12},{12,16},{16,20},{20,24},{24,28},{1,5},{5,9},{9,... | collective-permute-start | bytes 196616 | tf_op jit(solution)/shard_map/ppermute | solution.py:406
  53.5 17.8 %collective-permute-start.18 = (bf16[3,32,2176]{2,1,0:T(8,128)(2,1)S(1)}, bf16[3,32,2176]{2,1,0:T(8,128)(2,1)S(1)}, u32[]{:S(2)}, u32[]{:S(2)}) collective-permute-start(bf16[3,32,2176]{2,1,0:T(8,128)(2,1)S(1)} %collective-permute-done.16.refs_0_), channel_id=1, source_target_pairs={{0,1},{1,0},{2,3},{3,2},{4,5},{5,4},{6,7},{7,6},{8,9},{9,8},{10,11... | collective-permute-start | bytes 1253384 | tf_op jit(solution)/shard_map/ppermute | solution.py:29
  61.8 9.5 %collective-permute-start.19 = (bf16[3,32,2176]{2,1,0:T(8,128)(2,1)S(1)}, bf16[3,32,2176]{2,1,0:T(8,128)(2,1)S(1)}, u32[]{:S(2)}, u32[]{:S(2)}) collective-permute-start(bf16[3,32,2176]{2,1,0:T(8,128)(2,1)S(1)} %collective-permute-done.17.refs_1_), channel_id=1, source_target_pairs={{0,1},{1,0},{2,3},{3,2},{4,5},{5,4},{6,7},{7,6},{8,9},{9,8},{10,11... | collective-permute-start | bytes 1253384 | tf_op jit(solution)/shard_map/ppermute | solution.py:29
  69.4 18.8 %collective-permute-start.5 = (bf16[2,256,512]{2,1,0:T(8,128)(2,1)S(1)}, bf16[2,256,512]{2,1,0:T(8,128)(2,1)S(1)}, u32[]{:S(2)}, u32[]{:S(2)}) collective-permute-start(bf16[2,256,512]{2,1,0:T(8,128)(2,1)S(1)} %get-tuple-element.26), channel_id=1, source_target_pairs={{0,1},{1,0},{2,3},{3,2},{4,5},{5,4},{6,7},{7,6},{8,9},{9,8},{10,11... | collective-permute-start | bytes 1572872 | tf_op jit(solution)/shard_map/ppermute | solution.py:29
  71.3 8.7 %copy-start = (f32[4]{0:T(128)S(1)}, f32[4]{0:T(128)}, u32[]{:S(2)}) copy-start(f32[4]{0:T(128)} %sinks.1) | copy-start | bytes 52
  79.9 10.0 %collective-permute-start.20 = (bf16[2,384,512]{2,1,0:T(8,128)(2,1)S(1)}, bf16[2,384,512]{2,1,0:T(8,128)(2,1)S(1)}, u32[]{:S(2)}, u32[]{:S(2)}) collective-permute-start(bf16[2,384,512]{2,1,0:T(8,128)(2,1)S(1)} %get-tuple-element.33), channel_id=1, source_target_pairs={{0,1},{1,0},{2,3},{3,2},{4,5},{5,4},{6,7},{7,6},{8,9},{9,8},{10,11... | collective-permute-start | bytes 2359304 | tf_op jit(solution)/shard_map/ppermute | solution.py:29
  87.6 3.1 %collective-permute-start.1 = (bf16[2,128,2048]{2,1,0:T(8,128)(2,1)S(1)}, bf16[2,128,2048]{2,1,0:T(8,128)(2,1)S(1)}, u32[]{:S(2)}, u32[]{:S(2)}) collective-permute-start(bf16[2,128,2048]{2,1,0:T(8,128)(2,1)S(1)} %get-tuple-element.22), channel_id=1, source_target_pairs={{0,1},{1,0},{2,3},{3,2},{4,5},{5,4},{6,7},{7,6},{8,9},{9,8},{10,11... | collective-permute-start | bytes 3145736 | tf_op jit(solution)/shard_map/ppermute | solution.py:29
  88.3 19.9 %collective-permute-start.6 = (bf16[2,128,512]{2,1,0:T(8,128)(2,1)S(1)}, bf16[2,128,512]{2,1,0:T(8,128)(2,1)S(1)}, u32[]{:S(2)}, u32[]{:S(2)}) collective-permute-start(bf16[2,128,512]{2,1,0:T(8,128)(2,1)S(1)} %bitcast.46), channel_id=1, source_target_pairs={{0,2},{1,3},{2,0},{3,1},{4,6},{5,7},{6,4},{7,5},{8,10},{9,11},{10,... | collective-permute-start | bytes 786440 | tf_op jit(solution)/shard_map/ppermute | solution.py:29
  90.1 15.9 %collective-permute-start.21 = (bf16[3,128,512]{2,1,0:T(8,128)(2,1)S(1)}, bf16[3,128,512]{2,1,0:T(8,128)(2,1)S(1)}, u32[]{:S(2)}, u32[]{:S(2)}) collective-permute-start(bf16[3,128,512]{2,1,0:T(8,128)(2,1)S(1)} %bitcast.45), channel_id=1, source_target_pairs={{0,2},{1,3},{2,0},{3,1},{4,6},{5,7},{6,4},{7,5},{8,10},{9,11},{10,... | collective-permute-start | bytes 1179656 | tf_op jit(solution)/shard_map/ppermute | solution.py:29
  90.8 38.6 %collective-permute-start.2 = (bf16[128,2048]{1,0:T(8,128)(2,1)S(1)}, bf16[128,2048]{1,0:T(8,128)(2,1)S(1)}, u32[]{:S(2)}, u32[]{:S(2)}) collective-permute-start(bf16[128,2048]{1,0:T(8,128)(2,1)S(1)} %fusion.1), channel_id=1, source_target_pairs={{0,2},{1,3},{2,0},{3,1},{4,6},{5,7},{6,4},{7,5},{8,10},{9,11},{10,... | collective-permute-start | bytes 1572872 | tf_op jit(solution)/shard_map/ppermute | solution.py:29
  92.4 32.3 %collective-permute-start.15 = (bf16[3,128,512]{2,1,0:T(8,128)(2,1)S(1)}, bf16[3,128,512]{2,1,0:T(8,128)(2,1)S(1)}, u32[]{:S(2)}, u32[]{:S(2)}) collective-permute-start(bf16[3,128,512]{2,1,0:T(8,128)(2,1)S(1)} %bitcast.44), channel_id=1, source_target_pairs={{0,2},{1,3},{2,0},{3,1},{4,6},{5,7},{6,4},{7,5},{8,10},{9,11},{10,... | collective-permute-start | bytes 1179656 | tf_op jit(solution)/shard_map/ppermute | solution.py:29
  106.1 18.6 %collective-permute-start.22 = (bf16[3,128,512]{2,1,0:T(8,128)(2,1)S(1)}, bf16[3,128,512]{2,1,0:T(8,128)(2,1)S(1)}, u32[]{:S(2)}, u32[]{:S(2)}) collective-permute-start(bf16[3,128,512]{2,1,0:T(8,128)(2,1)S(1)} %add_convert_fusion.2), channel_id=1, source_target_pairs={{0,4},{1,5},{2,6},{3,7},{4,0},{5,1},{6,2},{7,3},{8,12},{9,13},{10,... | collective-permute-start | bytes 1179656 | tf_op jit(solution)/shard_map/ppermute | solution.py:29
  108.4 22.1 %collective-permute-start.7 = (bf16[128,512]{1,0:T(8,128)(2,1)S(1)}, bf16[128,512]{1,0:T(8,128)(2,1)S(1)}, u32[]{:S(2)}, u32[]{:S(2)}) collective-permute-start(bf16[128,512]{1,0:T(8,128)(2,1)S(1)} %slice_bitcast_fusion.3), channel_id=1, source_target_pairs={{0,4},{1,5},{2,6},{3,7},{4,0},{5,1},{6,2},{7,3},{8,12},{9,13},{10,... | collective-permute-start | bytes 393224 | tf_op jit(solution)/shard_map/ppermute | solution.py:29
  125.0 6.4 %collective-permute-start.23 = (bf16[128,512]{1,0:T(8,128)(2,1)S(1)}, bf16[128,512]{1,0:T(8,128)(2,1)S(1)}, u32[]{:S(2)}, u32[]{:S(2)}) collective-permute-start(bf16[128,512]{1,0:T(8,128)(2,1)S(1)} %get-tuple-element.42), channel_id=1, source_target_pairs={{0,8},{1,9},{2,10},{3,11},{4,12},{5,13},{6,14},{7,15},{8,0},{9,1},... | collective-permute-start | bytes 393224 | tf_op jit(solution)/shard_map/ppermute | solution.py:29
  125.1 12.8 %collective-permute-start.24 = (bf16[128,512]{1,0:T(8,128)(2,1)S(1)}, bf16[128,512]{1,0:T(8,128)(2,1)S(1)}, u32[]{:S(2)}, u32[]{:S(2)}) collective-permute-start(bf16[128,512]{1,0:T(8,128)(2,1)S(1)} %get-tuple-element.44), channel_id=1, source_target_pairs={{0,16},{1,17},{2,18},{3,19},{4,20},{5,21},{6,22},{7,23},{8,24},{9,... | collective-permute-start | bytes 393224 | tf_op jit(solution)/shard_map/ppermute | solution.py:29
  127.5 10.3 %collective-permute-start.25 = (bf16[128,512]{1,0:T(8,128)(2,1)S(1)}, bf16[128,512]{1,0:T(8,128)(2,1)S(1)}, u32[]{:S(2)}, u32[]{:S(2)}) collective-permute-start(bf16[128,512]{1,0:T(8,128)(2,1)S(1)} %get-tuple-element.43), channel_id=1, source_target_pairs={{0,24},{1,25},{2,26},{3,27},{4,28},{5,29},{6,30},{7,31},{8,16},{9,... | collective-permute-start | bytes 393224 | tf_op jit(solution)/shard_map/ppermute | solution.py:29

commit v2 on v1

--- a/solution.py
+++ b/solution.py
@@ -35,6 +35,10 @@
 
 def in_hbm(*values):
     return [pltpu.with_memory_space_constraint(value, pltpu.HBM) for value in values]
+
+
+def in_vmem(*values):
+    return [pltpu.with_memory_space_constraint(value, pltpu.VMEM) for value in values]
 
 
 def load(pairs, sems):
@@ -89,10 +93,11 @@
     last[...] = pairs[rows - BAND_LENGTH :, :]
 
 
-def attend_kernel(
-    meta, sinks, queries, pairs, before, source, send, keep, attended, output_w, sems
-):
-    (copy,) = load([(source, output_w)], sems)
+def attend_kernel(ahead, meta, sinks, queries, pairs, before, source, *refs):
+    (send, keep), (attended, output_w, sems) = refs[ahead : ahead + 2], refs[2 * ahead + 2 :]
+    copy, *early = load(
+        [(source, output_w), *zip(refs[:ahead], refs[ahead + 2 : 2 * ahead + 2])], sems
+    )
     rows, q_width = queries.shape
     width = pairs.shape[1] // 2
     groups = q_width // width
@@ -136,6 +141,8 @@
         out[k % half] = jnp.dot(
             attended[pl.ds(start, count), :], output_w[...], preferred_element_type=jnp.float32
         ).astype(jnp.bfloat16)
+    for copy in early:
+        copy.wait()
 
 
 def pack_kernel(experts, tp, meta, *refs):
@@ -210,41 +217,21 @@
 def expert_kernel(places, blocks, experts, shared, meta, *refs):
     pieces, refs = refs[: len(places)], refs[len(places) :]
     weights, refs = refs[: 6 if shared else 3], refs[6 if shared else 3 :]
-    send, keep, held, hidden = refs[:4]
-    stored, sems = refs[4:-1], refs[-1]
-    gate, up, down = stored[:3]
+    send, keep, held, hidden = refs
+    gate, up, down = weights[:3]
     exp_dev, width, units = gate.shape
     half, rows, slim = send.shape
     size = rows // blocks
     chunk = min(256, units)
     order = [(2 * k + 1 if k < half else 2 * (k - half)) for k in range(2 * half)]
     starts = [pl.multiple_of((meta[0] ^ g) * slim, slim) for g in order]
-    copies = {}
-
-    def fetch(key, number, part):
-        copies[key] = pltpu.make_async_copy(
-            weights[number].at[part], stored[number].at[part], sems.at[len(copies)]
-        )
-        copies[key].start()
-
-    whole = (slice(None), slice(None))
-    for j in range(exp_dev):
-        for c in range(0, units, chunk):
-            for number in (0, 1):
-                fetch((number, j, c), number, (j, slice(None), slice(c, c + chunk)))
-    if shared:
-        fetch("gate", 3, whole)
-        fetch("up", 4, whole)
-        fetch("down", 5, whole)
-    for k in range(2 * half):
-        fetch((2, k), 2, (slice(None), pl.ds(starts[k], slim)))
-
-    for piece, (first, xor, number) in zip(pieces, places):
+
+    for piece, (first, xor, number, col) in zip(pieces, places):
         part = piece.shape[1]
         where = 0 if xor is None else (meta[0] % number) ^ xor
         for b in range(piece.shape[0]):
             start = pl.multiple_of((first + b) * size + where * part, part)
-            held[pl.ds(start, part), :] = piece[b]
+            held[pl.ds(start, part), col : col + piece.shape[2]] = piece[b]
     several = max(n for n in (1, 2, 3) if blocks % n == 0)
     most = several * size
 
@@ -266,8 +253,6 @@
 
     for j in range(exp_dev):
         for c in range(0, units, chunk):
-            copies[0, j, c].wait()
-            copies[1, j, c].wait()
 
             def opening(at, j=j, c=c):
                 tokens = held[at, :width]
@@ -279,25 +264,22 @@
 
             over_rows(opening)
     if shared:
-        copies["gate"].wait()
-        copies["up"].wait()
         own = held[:size, :width]
         hidden_sh = (
-            silu(jnp.dot(own, stored[3][...], preferred_element_type=jnp.float32))
-            * jnp.dot(own, stored[4][...], preferred_element_type=jnp.float32)
+            silu(jnp.dot(own, weights[3][...], preferred_element_type=jnp.float32))
+            * jnp.dot(own, weights[4][...], preferred_element_type=jnp.float32)
         ).astype(jnp.bfloat16)
-        copies["down"].wait()
     for k in range(2 * half):
         out = send if k < half else keep
-        copies[2, k].wait()
 
         def closing(at, k=k, out=out):
+            rows_down = [down[j, :, pl.ds(starts[k], slim)] for j in range(exp_dev)]
             result = jnp.dot(
-                hidden[at, :], down[:, pl.ds(starts[k], slim)], preferred_element_type=jnp.float32
+                hidden[at, :], jnp.concatenate(rows_down, axis=0), preferred_element_type=jnp.float32
             )
             if shared:
                 extra = jnp.dot(
-                    hidden_sh, stored[5][:, pl.ds(starts[k], slim)], preferred_element_type=jnp.float32
+                    hidden_sh, weights[5][:, pl.ds(starts[k], slim)], preferred_element_type=jnp.float32
                 )
                 out[k % half, :size, :] = (result[:size] + extra).astype(jnp.bfloat16)
                 out[k % half, size:, :] = result[size:].astype(jnp.bfloat16)
@@ -311,19 +293,16 @@
     exp_dev, width, units = gate.shape
     tp = lax.axis_size("tp")
     rows = blocks * size
-    total = pieces[0].shape[-1]
-    weights = [gate, up, down.reshape(exp_dev * units, width), *shared]
+    total = width + -(-2 * experts // LANES) * LANES
+    weights = [gate, up, down, *shared]
     out = jax.ShapeDtypeStruct((tp // 2, rows, width // tp), jnp.bfloat16)
-    copies = 2 * exp_dev * (units // min(256, units)) + tp + len(shared)
     return pl.pallas_call(
         functools.partial(expert_kernel, tuple(places), blocks, experts, bool(shared)),
-        in_specs=[SMEM] + [VMEM] * len(pieces) + [HBM] * len(weights),
+        in_specs=[SMEM] + [VMEM] * (len(pieces) + len(weights)),
         out_specs=(VMEM, VMEM),
         scratch_shapes=[
             pltpu.VMEM((rows, total), jnp.bfloat16),
             pltpu.VMEM((rows, exp_dev * units), jnp.bfloat16),
-            *[pltpu.VMEM(w.shape, w.dtype) for w in weights],
-            pltpu.SemaphoreType.DMA((copies,)),
         ],
         out_shape=(out, out),
         cost_estimate=pl.CostEstimate(
@@ -331,8 +310,8 @@
             bytes_accessed=6 * width * units * exp_dev,
             transcendentals=rows * units * exp_dev,
         ),
-        compiler_params=limit(36),
-    )(meta, *pieces, *in_hbm(*weights))
+        compiler_params=limit(14 + (8 * rows * total >> 20)),
+    )(meta, *pieces, *in_vmem(*weights))
 
 
 def add_up(*parts):
@@ -397,7 +376,7 @@
             pltpu.SemaphoreType.DMA((4 + rows_first // min(128, rows_first),)),
         ],
         cost_estimate=pl.CostEstimate(flops=1 << 30, bytes_accessed=1 << 22, transcendentals=0),
-        compiler_params=limit(24),
+        compiler_params=limit(12),
         name="project",
     )(
         *in_hbm(tokens_first, attn_gain.reshape(1, -1), w_query, key_matrix, value_matrix),
@@ -406,20 +385,22 @@
     before = lax.ppermute(last, "ep", [(i, i + 1) for i in range(ep - 1)])
     count = rows_first // tp
     part = jax.ShapeDtypeStruct((lines, count, w_output.shape[1]), jnp.bfloat16)
-    outward, kept = pl.pallas_call(
-        attend_kernel,
-        out_shape=(part, part),
-        in_specs=[SMEM] * 2 + [VMEM] * 3 + [HBM],
-        out_specs=(VMEM,) * 2,
+    late = (w_gate_shared, w_up_shared, w_down_exp, w_down_shared)
+    outward, kept, *late = pl.pallas_call(
+        functools.partial(attend_kernel, len(late)),
+        out_shape=(part, part, *[pltpu.VMEM(w.shape, w.dtype) for w in late]),
+        in_specs=[SMEM] * 2 + [VMEM] * 3 + [HBM] * (1 + len(late)),
+        out_specs=(VMEM,) * (2 + len(late)),
         scratch_shapes=[
             pltpu.VMEM((rows_first, w_query.shape[1]), jnp.bfloat16),
             pltpu.VMEM(w_output.shape, jnp.bfloat16),
-            pltpu.SemaphoreType.DMA((1,)),
+            pltpu.SemaphoreType.DMA((1 + len(late),)),
         ],
         cost_estimate=pl.CostEstimate(flops=1 << 30, bytes_accessed=1 << 22, transcendentals=0),
-        compiler_params=limit(24),
+        compiler_params=limit(12),
         name="attend",
-    )(meta, head_sink_logit, queries, pairs, before, *in_hbm(w_output))
+    )(meta, head_sink_logit, queries, pairs, before, *in_hbm(w_output, *late))
+    gate_shared, up_shared, down, down_shared = late
     outward = swap(outward, 0, 1)
     mixer_out = add_up(
         outward[0],
@@ -428,42 +409,54 @@
     )
     along = join(around)
     across = swap(along, 1, 0)
-    rest_along, rest_across = [(along, 0)], [(across, 0)]
+    cut = along.shape[2] // LANES // 2 * LANES
+    rest_along, rest_across = [(along, 0, 0)], [(across, 0, 0)]
     for s in range(1, lines):
         other = swap(along, 0, s << 1)
-        rest_along.append((other, s << 1))
-        rest_across.append((swap(other, 1, 0), s << 1))
+        rest_along.append((other, s << 1, 0))
+        rest_across.append((swap(other[:, :, :cut], 1, 0), s << 1, 0))
+        rest_across.append((swap(across[:, :, cut:], 0, s << 1), s << 1, cut))
 
     def with_core(listed):
-        listed = listed + [(swap(v, 0, 1), x ^ 1) for v, x in listed]
-        return [v for v, _ in listed], [(0, x, tp) for _, x in listed]
-
-    near = ([whole[None], beside, swap(beside, 0, 1)], [(0, None, 1), (1, 0, 2), (1, 1, 2)])
-    shared = (w_gate_shared, w_up_shared, w_down_shared)
+        listed = listed + [(swap(v, 0, 1), x ^ 1, c) for v, x, c in listed]
+        return [v for v, _, _ in listed], [(0, x, tp, c) for _, x, c in listed]
+
+    near = ([whole[None], beside, swap(beside, 0, 1)], [(0, None, 1, 0), (1, 0, 2, 0), (1, 1, 2, 0)])
+    shared = (gate_shared, up_shared, down_shared)
     keep = []
     for name, (pieces, places), blocks, extra in (
         ("near", near, 2, shared),
+        ("across", with_core(rest_across), columns - 1, ()),
         ("along", with_core(rest_along), columns - 1, ()),
-        ("across", with_core(rest_across), columns - 1, ()),
     ):
         s, k = experts_call(
             meta, pieces, places, blocks, rows_second,
-            w_gate_exp, w_up_exp, w_down_exp, extra, experts,
+            w_gate_exp, w_up_exp, down, extra, experts,
         )
         slim = s.shape[-1]
         sent = swap(s, 0, 1).reshape(lines, blocks, rows_second, slim)
         kept = k.reshape(lines, blocks, rows_second, slim)
-        gone = [add_up(sent[i], kept[i]) for i in range(1, lines)]
-        if gone and name != "near":
-            meta, *gone = lax.optimization_barrier((meta, *gone))
-        out = [swap(gone[i - 1], 0, i << 1) for i in range(1, lines)]
-        keep.append(add_up(sent[0], kept[0], *out))
-    near, along, across = keep
-    far = swap(across, 1, 0)
-    beside = swap(near[1], 1, 0)
-    outgoing = add_up(along, far)
-    arrived = [swap(outgoing[s - 1], s << 1, 0) for s in range(1, columns)]
-    moe_out = add_up(near[0], beside, *arrived)
+        spans = [(0, blocks)] if name == "near" else [(1, blocks), (0, 1)]
+        gone = [[add_up(sent[i, a:b], kept[i, a:b]) for a, b in spans] for i in range(1, lines)]
+        if gone and name == "across":
+            meta, gone = lax.optimization_barrier((meta, gone))
+        out = [[swap(value, 0, i << 1) for value in gone[i - 1]] for i in range(1, lines)]
+        keep.append(
+            [
+                add_up(sent[0, a:b], kept[0, a:b], *[o[n] for o in out])
+                for n, (a, b) in enumerate(spans)
+            ]
+        )
+    near, across, along = keep
+    far = [swap(value, 1, 0) for value in across]
+    outgoing = [add_up(along[0], far[0])]
+    outgoing.append(add_up(along[1], far[1]))
+    arrived = [
+        swap(outgoing[0][s - 2] if s > 1 else outgoing[1][0], s << 1, 0)
+        for s in [*range(2, columns), 1]
+    ]
+    beside = swap(near[0][1], 1, 0)
+    moe_out = add_up(near[0][0], beside, *arrived)
     return (mixer_out, moe_out)
 
 

time: 139 us -> 132 us (0.950)
  starting transfers between devices: 26.8 us -> 34.9 us
  Pallas kernels: 39 us -> 32 us
  waiting for transfers between devices: 66.8 us -> 59.8 us
    ppermute x25 -> x30, waiting for transfers between devices: 66.8 us -> 58.1 us  [swap(): return lax.ppermute(value, ('ep', 'tp'), pairs)]
    pallas_call x3, Pallas kernels: 24.6 us -> 16.4 us  [experts_call(): pl.pallas_call(functools.partial(expert_kernel, tuple(places), blocks, ex...]
    ppermute x25 -> x30, starting transfers between devices: 23.2 us -> 31.3 us  [swap(): return lax.ppermute(value, ('ep', 'tp'), pairs)]
    ppermute x1, waiting for transfers between devices: 0.01 us -> 1.7 us  [local(): before = lax.ppermute(last, 'ep', [(i, i + 1) for i in range(ep - 1)])]
  transfers between devices with their start and end apart: 26 -> 31, of which waited for: 11 -> 14; matrix products, arithmetic and copies ran while one was open for 3% -> 2% of each run, Pallas kernels for 27% -> 23%
where the time goes in v2:
time: 132 us; the launch traced here: 131 us
  waiting for transfers between devices  59.8 us (45%)
  starting transfers between devices  34.9 us (26%)
  Pallas kernels  32 us (24%)
  other arithmetic  3.74 us (3%)
    ppermute x30, waiting for transfers between devices, swap(): return lax.ppermute(value, ('ep', 'tp'), pairs)  58.1 us
    ppermute x30, starting transfers between devices, swap(): return lax.ppermute(value, ('ep', 'tp'), pairs)  31.3 us
    pallas_call x3, Pallas kernels, experts_call(): pl.pallas_call(functools.partial(expert_kernel, tuple(places), blocks, ex...  16.4 us
    pallas_call x1, Pallas kernels, local(): pl.pallas_call(functools.partial(attend_kernel, len(late)), out_shape=(pa...  8.88 us
    pallas_call x1, Pallas kernels, local(): pl.pallas_call(project_kernel, out_shape=(jax.ShapeDtypeStruct((rows_firs...  4.82 us
    ppermute x1, starting transfers between devices, local(): before = lax.ppermute(last, 'ep', [(i, i + 1) for i in range(ep - 1)])  3.57 us
  transfers between devices with their start and end apart: 31, of which 14 were waited for; matrix products, arithmetic and copies ran while one was open for 2% of the time, Pallas kernels for 23%

profile of v2, /device:TPU:0, one launch (start us, length us, event | category | flops | bytes accessed | tf_op | source)
XLA Modules:
  0.0 131.5 jit_solution(5436901804852854232)
XLA Ops:
  0.7 1.9 %pack.1 = (bf16[128,2176]{1,0:T(8,128)(2,1)S(1)}, bf16[64,2176]{1,0:T(8,128)(2,1)S(1)}, bf16[32,2176]{1,0:T(8,128)(2,1)S(1)}) custom-call(s32[3]{0:T(128)S(1)} %pad_add_fusion.meta, bf16[128,2048]{1,0:T(8,128)(2,1)} %refs_0_.5, f32[1,2048]{1,0:T(1,128)} %bitcast.83, s32[4,128]{1,0:T(4,128)} %bitcast.85, f32[4,128]{1,0:T(4,128)} %bitcast.86), custom_call_target="tpu_custom_call" | custom-call | flops 67108864 | bytes 1048576 | tf_op jit(solution)/shard_map/pack/pallas_call | solution.py:176
  2.6 5.1 %collective-permute-start.10 = (bf16[32,2176]{1,0:T(8,128)(2,1)S(1)}, bf16[32,2176]{1,0:T(8,128)(2,1)S(1)}, u32[]{:S(2)}, u32[]{:S(2)}) collective-permute-start(bf16[32,2176]{1,0:T(8,128)(2,1)S(1)} %get-tuple-element.36), channel_id=1, source_target_pairs={{0,24},{1,25},{2,26},{3,27},{4,28},{5,29},{6,30},{7,31},{8,16},{9,... | collective-permute-start | bytes 417800 | tf_op jit(solution)/shard_map/ppermute | solution.py:29
  7.8 0.6 collective-permute-start.9
  8.4 3.9 %collective-permute-done.10.refs_2_ = bf16[32,2176]{1,0:T(8,128)(2,1)S(1)} collective-permute-done((bf16[32,2176]{1,0:T(8,128)(2,1)S(1)}, bf16[32,2176]{1,0:T(8,128)(2,1)S(1)}, u32[]{:S(2)}, u32[]{:S(2)}) %collective-permute-start.10) | collective-permute-done | bytes 139296 | tf_op jit(solution)/shard_map/ppermute | solution.py:29
  12.3 3.2 %collective-permute-done.8.refs_0_ = bf16[32,2176]{1,0:T(8,128)(2,1)S(1)} collective-permute-done((bf16[32,2176]{1,0:T(8,128)(2,1)S(1)}, bf16[32,2176]{1,0:T(8,128)(2,1)S(1)}, u32[]{:S(2)}, u32[]{:S(2)}) %collective-permute-start.8) | collective-permute-done | bytes 139296 | tf_op jit(solution)/shard_map/ppermute | solution.py:29
  15.5 4.0 %collective-permute-done.9.refs_1_ = bf16[32,2176]{1,0:T(8,128)(2,1)S(1)} collective-permute-done((bf16[32,2176]{1,0:T(8,128)(2,1)S(1)}, bf16[32,2176]{1,0:T(8,128)(2,1)S(1)}, u32[]{:S(2)}, u32[]{:S(2)}) %collective-permute-start.9) | collective-permute-done | bytes 139296 | tf_op jit(solution)/shard_map/ppermute | solution.py:29
  19.6 1.6 %collective-permute-start.11 = (bf16[3,32,2176]{2,1,0:T(8,128)(2,1)S(1)}, bf16[3,32,2176]{2,1,0:T(8,128)(2,1)S(1)}, u32[]{:S(2)}, u32[]{:S(2)}) collective-permute-start(bf16[3,32,2176]{2,1,0:T(8,128)(2,1)S(1)} %join.1.refs_0_), channel_id=1, source_target_pairs={{0,4},{1,5},{2,6},{3,7},{4,0},{5,1},{6,2},{7,3},{8,12},{9,13},{10,... | collective-permute-start | bytes 1253384 | tf_op jit(solution)/shard_map/ppermute | solution.py:29
  21.1 1.5 %collective-permute-start.12 = (bf16[3,32,2176]{2,1,0:T(8,128)(2,1)S(1)}, bf16[3,32,2176]{2,1,0:T(8,128)(2,1)S(1)}, u32[]{:S(2)}, u32[]{:S(2)}) collective-permute-start(bf16[3,32,2176]{2,1,0:T(8,128)(2,1)S(1)} %join.1.refs_0_), channel_id=1, source_target_pairs={{0,2},{1,3},{2,0},{3,1},{4,6},{5,7},{6,4},{7,5},{8,10},{9,11},{10,... | collective-permute-start | bytes 1253384 | tf_op jit(solution)/shard_map/ppermute | solution.py:29
  22.6 0.5 collective-permute-start.3
  23.3 8.9 %collective-permute-done.11.refs_0_ = bf16[3,32,2176]{2,1,0:T(8,128)(2,1)S(1)} collective-permute-done((bf16[3,32,2176]{2,1,0:T(8,128)(2,1)S(1)}, bf16[3,32,2176]{2,1,0:T(8,128)(2,1)S(1)}, u32[]{:S(2)}, u32[]{:S(2)}) %collective-permute-start.11) | collective-permute-done | bytes 417824 | tf_op jit(solution)/shard_map/ppermute | solution.py:29
  32.2 1.6 %collective-permute-start.14 = (bf16[3,32,1152]{2,1,0:T(8,128)(2,1)S(1)}, bf16[3,32,1152]{2,1,0:T(8,128)(2,1)S(1)}, u32[]{:S(2)}, u32[]{:S(2)}) collective-permute-start(bf16[3,32,1152]{2,1,0:T(8,128)(2,1)S(1)} %slice.131), channel_id=1, source_target_pairs={{0,2},{1,3},{2,0},{3,1},{4,6},{5,7},{6,4},{7,5},{8,10},{9,11},{10,... | collective-permute-start | bytes 663560 | tf_op jit(solution)/shard_map/ppermute | solution.py:29
  33.8 1.6 %collective-permute-start.13 = (bf16[3,32,1024]{2,1,0:T(8,128)(2,1)S(1)}, bf16[3,32,1024]{2,1,0:T(8,128)(2,1)S(1)}, u32[]{:S(2)}, u32[]{:S(2)}) collective-permute-start(bf16[3,32,1024]{2,1,0:T(8,128)(2,1)S(1)} %slice.130), channel_id=1, source_target_pairs={{0,4},{1,5},{2,6},{3,7},{4,0},{5,1},{6,2},{7,3},{8,12},{9,13},{10,... | collective-permute-start | bytes 589832 | tf_op jit(solution)/shard_map/ppermute | solution.py:29
  35.3 1.0 multiply_sine_fusion
  36.3 4.2 %collective-permute-done.13.refs_1_ = bf16[3,32,1024]{2,1,0:T(8,128)(2,1)S(1)} collective-permute-done((bf16[3,32,1024]{2,1,0:T(8,128)(2,1)S(1)}, bf16[3,32,1024]{2,1,0:T(8,128)(2,1)S(1)}, u32[]{:S(2)}, u32[]{:S(2)}) %collective-permute-start.13) | collective-permute-done | bytes 196640 | tf_op jit(solution)/shard_map/ppermute | solution.py:29
  40.5 0.5 collective-permute-start.17
  41.0 4.8 %project.1 = (bf16[512,256]{1,0:T(8,128)(2,1)S(1)}, bf16[512,256]{1,0:T(8,128)(2,1)S(1)}, bf16[128,256]{1,0:T(8,128)(2,1)S(1)}) custom-call(bf16[512,2048]{1,0:T(8,128)(2,1)} %refs_0_.3, f32[1,2048]{1,0:T(1,128)} %bitcast.84, bf16[2048,256]{1,0:T(8,128)(2,1)} %refs_2_.2, bf16[2048,128]{1,0:T(8,128)(2,1)} %refs_3_.3, bf16[2048,128]{1,0:T(8,128)(2,1)} %refs_4_.3, ...), custom_call_target="tpu_custom_call" | custom-call | flops 1073741824 | bytes 4194304 | tf_op jit(solution)/shard_map/project/pallas_call | solution.py:361
  45.9 3.6 %collective-permute-start = (bf16[128,256]{1,0:T(8,128)(2,1)S(1)}, bf16[128,256]{1,0:T(8,128)(2,1)S(1)}, u32[]{:S(2)}, u32[]{:S(2)}) collective-permute-start(bf16[128,256]{1,0:T(8,128)(2,1)S(1)} %get-tuple-element.25), channel_id=1, source_target_pairs={{0,4},{4,8},{8,12},{12,16},{16,20},{20,24},{24,28},{1,5},{5,9},{9,... | collective-permute-start | bytes 196616 | tf_op jit(solution)/shard_map/ppermute | solution.py:385
  49.4 1.7 %collective-permute-done.before = bf16[128,256]{1,0:T(8,128)(2,1)S(1)} collective-permute-done((bf16[128,256]{1,0:T(8,128)(2,1)S(1)}, bf16[128,256]{1,0:T(8,128)(2,1)S(1)}, u32[]{:S(2)}, u32[]{:S(2)}) %collective-permute-start) | collective-permute-done | bytes 65568 | tf_op jit(solution)/shard_map/ppermute | solution.py:385
  51.2 8.9 %attend.1 = (bf16[2,128,2048]{2,1,0:T(8,128)(2,1)S(1)}, bf16[2,128,2048]{2,1,0:T(8,128)(2,1)S(1)}, bf16[2048,256]{1,0:T(8,128)(2,1)S(1)}, bf16[2048,256]{1,0:T(8...) custom-call(s32[3]{0:T(128)S(1)} %pad_add_fusion.meta, f32[4]{0:T(128)S(1)} %copy-done.2, ...), custom_call_target="tpu_custom_call" | custom-call | flops 1073741824 | bytes 4194304 | tf_op jit(solution)/shard_map/attend/pallas_call | solution.py:389
  60.2 5.8 %shard_map.177 = (bf16[2,384,512]{2,1,0:T(8,128)(2,1)S(1)}, bf16[2,384,512]{2,1,0:T(8,128)(2,1)S(1)}) custom-call(s32[3]{0:T(128)S(1)} %pad_add_fusion.meta, bf16[3,32,2176]{2,1,0:T(8,128)(2,1)S(1)} %collective-permute-done.11.refs_0_, bf16[3,32,1024]{2,1,0:T(8,128)(2,1)S(1)} %collective-permute-done.13.refs_1_, ...), custom_call_target="tpu_custom_call" | custom-call | flops 4831838208 | bytes 12582912 | tf_op jit(solution)/shard_map/pallas_call | solution.py:299
  66.0 0.5 collective-permute-start.18
  66.6 4.6 %shard_map.176 = (bf16[2,256,512]{2,1,0:T(8,128)(2,1)S(1)}, bf16[2,256,512]{2,1,0:T(8,128)(2,1)S(1)}) custom-call(s32[3]{0:T(128)S(1)} %pad_add_fusion.meta, bf16[1,128,2176]{2,1,0:T(8,128)(2,1)S(1)} %bitcast.70, bf16[1,64,2176]{2,1,0:T(8,128)(2,1)S(1)} %bitcast.72, bf16[1,64,2176]{2,1,0:T(8,128)(2,1)S(1)} %collective-permute-done.4.refs_2_, ...), custom_call_target="tpu_custom_call" | custom-call | flops 3221225472 | bytes 12582912 | tf_op jit(solution)/shard_map/pallas_call | solution.py:299
  71.2 0.5 collective-permute-start.1
  71.8 0.4 collective-permute-start.20
  72.2 0.9 collective-permute-done.5
  73.2 1.6 %collective-permute-start.6 = (bf16[2,128,512]{2,1,0:T(8,128)(2,1)S(1)}, bf16[2,128,512]{2,1,0:T(8,128)(2,1)S(1)}, u32[]{:S(2)}, u32[]{:S(2)}) collective-permute-start(bf16[2,128,512]{2,1,0:T(8,128)(2,1)S(1)} %bitcast.82), channel_id=1, source_target_pairs={{0,2},{1,3},{2,0},{3,1},{4,6},{5,7},{6,4},{7,5},{8,10},{9,11},{10,... | collective-permute-start | bytes 786440 | tf_op jit(solution)/shard_map/ppermute | solution.py:29
  74.9 0.3 collective-permute-done.19.refs_2_
  75.2 0.6 collective-permute-done.20.refs_3_
  75.8 6.0 %shard_map.178 = (bf16[2,384,512]{2,1,0:T(8,128)(2,1)S(1)}, bf16[2,384,512]{2,1,0:T(8,128)(2,1)S(1)}) custom-call(s32[3]{0:T(128)S(1)} %pad_add_fusion.meta, bf16[3,32,2176]{2,1,0:T(8,128)(2,1)S(1)} %join.1.refs_0_, bf16[3,32,2176]{2,1,0:T(8,128)(2,1)S(1)} %collective-permute-done.12.refs_1_, bf16[3,32,2176]{2,1,0:T(8,128)(2,1)S(1)} %collective-permute-done.19.refs_2_, ...), custom_call_target="tpu_custom_call" | custom-call | flops 4831838208 | bytes 12582912 | tf_op jit(solution)/shard_map/pallas_call | solution.py:299
  81.8 0.2 collective-permute-start.21
  82.2 1.6 %collective-permute-start.2 = (bf16[128,2048]{1,0:T(8,128)(2,1)S(1)}, bf16[128,2048]{1,0:T(8,128)(2,1)S(1)}, u32[]{:S(2)}, u32[]{:S(2)}) collective-permute-start(bf16[128,2048]{1,0:T(8,128)(2,1)S(1)} %fusion.1), channel_id=1, source_target_pairs={{0,2},{1,3},{2,0},{3,1},{4,6},{5,7},{6,4},{7,5},{8,10},{9,11},{10,... | collective-permute-start | bytes 1572872 | tf_op jit(solution)/shard_map/ppermute | solution.py:29
  83.8 0.5 collective-permute-start.23
  84.3 1.5 %collective-permute-start.28 = (bf16[1,128,512]{2,1,0:T(8,128)(2,1)S(1)}, bf16[1,128,512]{2,1,0:T(8,128)(2,1)S(1)}, u32[]{:S(2)}, u32[]{:S(2)}) collective-permute-start(bf16[1,128,512]{2,1,0:T(8,128)(2,1)S(1)} %fusion.12), channel_id=1, source_target_pairs={{0,2},{1,3},{2,0},{3,1},{4,6},{5,7},{6,4},{7,5},{8,10},{9,11},{10,... | collective-permute-start | bytes 393224 | tf_op jit(solution)/shard_map/ppermute | solution.py:29
  85.9 19.0 %collective-permute-done.28 = bf16[1,128,512]{2,1,0:T(8,128)(2,1)S(1)} collective-permute-done((bf16[1,128,512]{2,1,0:T(8,128)(2,1)S(1)}, bf16[1,128,512]{2,1,0:T(8,128)(2,1)S(1)}, u32[]{:S(2)}, u32[]{:S(2)}) %collective-permute-start.28) | collective-permute-done | bytes 131104 | tf_op jit(solution)/shard_map/ppermute | solution.py:29
  104.9 2.4 %collective-permute-start.29 = (bf16[1,128,512]{2,1,0:T(8,128)(2,1)S(1)}, bf16[1,128,512]{2,1,0:T(8,128)(2,1)S(1)}, u32[]{:S(2)}, u32[]{:S(2)}) collective-permute-start(bf16[1,128,512]{2,1,0:T(8,128)(2,1)S(1)} %fusion.10), channel_id=1, source_target_pairs={{0,4},{1,5},{2,6},{3,7},{4,0},{5,1},{6,2},{7,3},{8,12},{9,13},{10,... | collective-permute-start | bytes 393224 | tf_op jit(solution)/shard_map/ppermute | solution.py:29
  107.7 1.6 %collective-permute-start.22 = (bf16[2,128,512]{2,1,0:T(8,128)(2,1)S(1)}, bf16[2,128,512]{2,1,0:T(8,128)(2,1)S(1)}, u32[]{:S(2)}, u32[]{:S(2)}) collective-permute-start(bf16[2,128,512]{2,1,0:T(8,128)(2,1)S(1)} %fusion.5), channel_id=1, source_target_pairs={{0,2},{1,3},{2,0},{3,1},{4,6},{5,7},{6,4},{7,5},{8,10},{9,11},{10,... | collective-permute-start | bytes 786440 | tf_op jit(solution)/shard_map/ppermute | solution.py:29
  109.3 0.5 collective-permute-start.27
  109.8 1.9 %collective-permute-done.29 = bf16[1,128,512]{2,1,0:T(8,128)(2,1)S(1)} collective-permute-done((bf16[1,128,512]{2,1,0:T(8,128)(2,1)S(1)}, bf16[1,128,512]{2,1,0:T(8,128)(2,1)S(1)}, u32[]{:S(2)}, u32[]{:S(2)}) %collective-permute-start.29) | collective-permute-done | bytes 131104 | tf_op jit(solution)/shard_map/ppermute | solution.py:29
  111.7 2.0 %collective-permute-start.7 = (bf16[128,512]{1,0:T(8,128)(2,1)S(1)}, bf16[128,512]{1,0:T(8,128)(2,1)S(1)}, u32[]{:S(2)}, u32[]{:S(2)}) collective-permute-start(bf16[128,512]{1,0:T(8,128)(2,1)S(1)} %slice_bitcast_fusion.2), channel_id=1, source_target_pairs={{0,4},{1,5},{2,6},{3,7},{4,0},{5,1},{6,2},{7,3},{8,12},{9,13},{10,... | collective-permute-start | bytes 393224 | tf_op jit(solution)/shard_map/ppermute | solution.py:29
  113.7 4.3 %collective-permute-done.27 = bf16[1,128,512]{2,1,0:T(8,128)(2,1)S(1)} collective-permute-done((bf16[1,128,512]{2,1,0:T(8,128)(2,1)S(1)}, bf16[1,128,512]{2,1,0:T(8,128)(2,1)S(1)}, u32[]{:S(2)}, u32[]{:S(2)}) %collective-permute-start.27) | collective-permute-done | bytes 131104 | tf_op jit(solution)/shard_map/ppermute | solution.py:29
  118.1 1.3 collective-permute-start.30
  119.3 0.1 add_convert_fusion.1
  119.5 2.0 %collective-permute-start.25 = (bf16[128,512]{1,0:T(8,128)(2,1)S(1)}, bf16[128,512]{1,0:T(8,128)(2,1)S(1)}, u32[]{:S(2)}, u32[]{:S(2)}) collective-permute-start(bf16[128,512]{1,0:T(8,128)(2,1)S(1)} %get-tuple-element.46), channel_id=1, source_target_pairs={{0,16},{1,17},{2,18},{3,19},{4,20},{5,21},{6,22},{7,23},{8,24},{9,... | collective-permute-start | bytes 393224 | tf_op jit(solution)/shard_map/ppermute | solution.py:29
  121.5 1.2 collective-permute-start.26
  122.8 1.0 fusion
  123.8 0.7 collective-permute-done.30
  124.5 6.2 %collective-permute-done.25 = bf16[128,512]{1,0:T(8,128)(2,1)S(1)} collective-permute-done((bf16[128,512]{1,0:T(8,128)(2,1)S(1)}, bf16[128,512]{1,0:T(8,128)(2,1)S(1)}, u32[]{:S(2)}, u32[]{:S(2)}) %collective-permute-start.25) | collective-permute-done | bytes 131104 | tf_op jit(solution)/shard_map/ppermute | solution.py:29
  130.7 0.7 fusion.9
  (50 shorter events, 1.4 us)
Async XLA Ops:
  0.6 50.5 %copy-start.2 = (f32[4]{0:T(128)S(1)}, f32[4]{0:T(128)}, u32[]{:S(2)}) copy-start(f32[4]{0:T(128)} %sinks.1) | copy-start | bytes 52
  2.6 9.7 %collective-permute-start.10 = (bf16[32,2176]{1,0:T(8,128)(2,1)S(1)}, bf16[32,2176]{1,0:T(8,128)(2,1)S(1)}, u32[]{:S(2)}, u32[]{:S(2)}) collective-permute-start(bf16[32,2176]{1,0:T(8,128)(2,1)S(1)} %get-tuple-element.36), channel_id=1, source_target_pairs={{0,24},{1,25},{2,26},{3,27},{4,28},{5,29},{6,30},{7,31},{8,16},{9,... | collective-permute-start | bytes 417800 | tf_op jit(solution)/shard_map/ppermute | solution.py:29
  7.7 7.8 %collective-permute-start.8 = (bf16[32,2176]{1,0:T(8,128)(2,1)S(1)}, bf16[32,2176]{1,0:T(8,128)(2,1)S(1)}, u32[]{:S(2)}, u32[]{:S(2)}) collective-permute-start(bf16[32,2176]{1,0:T(8,128)(2,1)S(1)} %get-tuple-element.36), channel_id=1, source_target_pairs={{0,8},{1,9},{2,10},{3,11},{4,12},{5,13},{6,14},{7,15},{8,0},{9,1},... | collective-permute-start | bytes 417800 | tf_op jit(solution)/shard_map/ppermute | solution.py:29
  7.8 11.8 %collective-permute-start.9 = (bf16[32,2176]{1,0:T(8,128)(2,1)S(1)}, bf16[32,2176]{1,0:T(8,128)(2,1)S(1)}, u32[]{:S(2)}, u32[]{:S(2)}) collective-permute-start(bf16[32,2176]{1,0:T(8,128)(2,1)S(1)} %get-tuple-element.36), channel_id=1, source_target_pairs={{0,16},{1,17},{2,18},{3,19},{4,20},{5,21},{6,22},{7,23},{8,24},{9,... | collective-permute-start | bytes 417800 | tf_op jit(solution)/shard_map/ppermute | solution.py:29
  19.6 12.6 %collective-permute-start.11 = (bf16[3,32,2176]{2,1,0:T(8,128)(2,1)S(1)}, bf16[3,32,2176]{2,1,0:T(8,128)(2,1)S(1)}, u32[]{:S(2)}, u32[]{:S(2)}) collective-permute-start(bf16[3,32,2176]{2,1,0:T(8,128)(2,1)S(1)} %join.1.refs_0_), channel_id=1, source_target_pairs={{0,4},{1,5},{2,6},{3,7},{4,0},{5,1},{6,2},{7,3},{8,12},{9,13},{10,... | collective-permute-start | bytes 1253384 | tf_op jit(solution)/shard_map/ppermute | solution.py:29
  21.1 12.6 %collective-permute-start.12 = (bf16[3,32,2176]{2,1,0:T(8,128)(2,1)S(1)}, bf16[3,32,2176]{2,1,0:T(8,128)(2,1)S(1)}, u32[]{:S(2)}, u32[]{:S(2)}) collective-permute-start(bf16[3,32,2176]{2,1,0:T(8,128)(2,1)S(1)} %join.1.refs_0_), channel_id=1, source_target_pairs={{0,2},{1,3},{2,0},{3,1},{4,6},{5,7},{6,4},{7,5},{8,10},{9,11},{10,... | collective-permute-start | bytes 1253384 | tf_op jit(solution)/shard_map/ppermute | solution.py:29
  22.6 37.4 %collective-permute-start.3 = (bf16[64,2176]{1,0:T(8,128)(2,1)S(1)}, bf16[64,2176]{1,0:T(8,128)(2,1)S(1)}, u32[]{:S(2)}, u32[]{:S(2)}) collective-permute-start(bf16[64,2176]{1,0:T(8,128)(2,1)S(1)} %get-tuple-element.29), channel_id=1, source_target_pairs={{0,4},{1,5},{2,6},{3,7},{4,0},{5,1},{6,2},{7,3},{8,12},{9,13},{10,... | collective-permute-start | bytes 835592 | tf_op jit(solution)/shard_map/ppermute | solution.py:29
  32.2 8.4 %collective-permute-start.14 = (bf16[3,32,1152]{2,1,0:T(8,128)(2,1)S(1)}, bf16[3,32,1152]{2,1,0:T(8,128)(2,1)S(1)}, u32[]{:S(2)}, u32[]{:S(2)}) collective-permute-start(bf16[3,32,1152]{2,1,0:T(8,128)(2,1)S(1)} %slice.131), channel_id=1, source_target_pairs={{0,2},{1,3},{2,0},{3,1},{4,6},{5,7},{6,4},{7,5},{8,10},{9,11},{10,... | collective-permute-start | bytes 663560 | tf_op jit(solution)/shard_map/ppermute | solution.py:29
  33.8 6.8 %collective-permute-start.13 = (bf16[3,32,1024]{2,1,0:T(8,128)(2,1)S(1)}, bf16[3,32,1024]{2,1,0:T(8,128)(2,1)S(1)}, u32[]{:S(2)}, u32[]{:S(2)}) collective-permute-start(bf16[3,32,1024]{2,1,0:T(8,128)(2,1)S(1)} %slice.130), channel_id=1, source_target_pairs={{0,4},{1,5},{2,6},{3,7},{4,0},{5,1},{6,2},{7,3},{8,12},{9,13},{10,... | collective-permute-start | bytes 589832 | tf_op jit(solution)/shard_map/ppermute | solution.py:29
  35.3 24.8 %collective-permute-start.15 = (bf16[3,32,2176]{2,1,0:T(8,128)(2,1)S(1)}, bf16[3,32,2176]{2,1,0:T(8,128)(2,1)S(1)}, u32[]{:S(2)}, u32[]{:S(2)}) collective-permute-start(bf16[3,32,2176]{2,1,0:T(8,128)(2,1)S(1)} %collective-permute-done.11.refs_0_), channel_id=1, source_target_pairs={{0,1},{1,0},{2,3},{3,2},{4,5},{5,4},{6,7},{7,6},{8,9},{9,8},{10,11... | collective-permute-start | bytes 1253384 | tf_op jit(solution)/shard_map/ppermute | solution.py:29
  40.5 19.6 %collective-permute-start.16 = (bf16[3,32,1024]{2,1,0:T(8,128)(2,1)S(1)}, bf16[3,32,1024]{2,1,0:T(8,128)(2,1)S(1)}, u32[]{:S(2)}, u32[]{:S(2)}) collective-permute-start(bf16[3,32,1024]{2,1,0:T(8,128)(2,1)S(1)} %collective-permute-done.13.refs_1_), channel_id=1, source_target_pairs={{0,1},{1,0},{2,3},{3,2},{4,5},{5,4},{6,7},{7,6},{8,9},{9,8},{10,11... | collective-permute-start | bytes 589832 | tf_op jit(solution)/shard_map/ppermute | solution.py:29
  40.5 19.6 %collective-permute-start.17 = (bf16[3,32,1152]{2,1,0:T(8,128)(2,1)S(1)}, bf16[3,32,1152]{2,1,0:T(8,128)(2,1)S(1)}, u32[]{:S(2)}, u32[]{:S(2)}) collective-permute-start(bf16[3,32,1152]{2,1,0:T(8,128)(2,1)S(1)} %collective-permute-done.14.refs_2_), channel_id=1, source_target_pairs={{0,1},{1,0},{2,3},{3,2},{4,5},{5,4},{6,7},{7,6},{8,9},{9,8},{10,11... | collective-permute-start | bytes 663560 | tf_op jit(solution)/shard_map/ppermute | solution.py:29
  45.9 5.3 %collective-permute-start = (bf16[128,256]{1,0:T(8,128)(2,1)S(1)}, bf16[128,256]{1,0:T(8,128)(2,1)S(1)}, u32[]{:S(2)}, u32[]{:S(2)}) collective-permute-start(bf16[128,256]{1,0:T(8,128)(2,1)S(1)} %get-tuple-element.25), channel_id=1, source_target_pairs={{0,4},{4,8},{8,12},{12,16},{16,20},{20,24},{24,28},{1,5},{5,9},{9,... | collective-permute-start | bytes 196616 | tf_op jit(solution)/shard_map/ppermute | solution.py:385
  51.2 9.0 %copy-start = (bf16[2,2048,512]{2,1,0:T(8,128)(2,1)S(1)}, bf16[2,2048,512]{2,1,0:T(8,128)(2,1)}, u32[]{:S(2)}) copy-start(bf16[2,2048,512]{2,1,0:T(8,128)(2,1)} %refs_4_.5) | copy-start | bytes 12582916
  51.2 9.0 %copy-start.1 = (bf16[2,2048,512]{2,1,0:T(8,128)(2,1)S(1)}, bf16[2,2048,512]{2,1,0:T(8,128)(2,1)}, u32[]{:S(2)}) copy-start(bf16[2,2048,512]{2,1,0:T(8,128)(2,1)} %refs_5_.1) | copy-start | bytes 12582916
  60.1 6.5 %collective-permute-start.4 = (bf16[1,64,2176]{2,1,0:T(8,128)(2,1)S(1)}, bf16[1,64,2176]{2,1,0:T(8,128)(2,1)S(1)}, u32[]{:S(2)}, u32[]{:S(2)}) collective-permute-start(bf16[1,64,2176]{2,1,0:T(8,128)(2,1)S(1)} %bitcast.71), channel_id=1, source_target_pairs={{0,1},{1,0},{2,3},{3,2},{4,5},{5,4},{6,7},{7,6},{8,9},{9,8},{10,11... | collective-permute-start | bytes 835592 | tf_op jit(solution)/shard_map/ppermute | solution.py:29
  66.0 8.8 %collective-permute-start.18 = (bf16[2,384,512]{2,1,0:T(8,128)(2,1)S(1)}, bf16[2,384,512]{2,1,0:T(8,128)(2,1)S(1)}, u32[]{:S(2)}, u32[]{:S(2)}) collective-permute-start(bf16[2,384,512]{2,1,0:T(8,128)(2,1)S(1)} %get-tuple-element.37), channel_id=1, source_target_pairs={{0,1},{1,0},{2,3},{3,2},{4,5},{5,4},{6,7},{7,6},{8,9},{9,8},{10,11... | collective-permute-start | bytes 2359304 | tf_op jit(solution)/shard_map/ppermute | solution.py:29
  71.1 2.0 %collective-permute-start.5 = (bf16[2,256,512]{2,1,0:T(8,128)(2,1)S(1)}, bf16[2,256,512]{2,1,0:T(8,128)(2,1)S(1)}, u32[]{:S(2)}, u32[]{:S(2)}) collective-permute-start(bf16[2,256,512]{2,1,0:T(8,128)(2,1)S(1)} %get-tuple-element.34), channel_id=1, source_target_pairs={{0,1},{1,0},{2,3},{3,2},{4,5},{5,4},{6,7},{7,6},{8,9},{9,8},{10,11... | collective-permute-start | bytes 1572872 | tf_op jit(solution)/shard_map/ppermute | solution.py:29
  71.2 10.8 %collective-permute-start.1 = (bf16[2,128,2048]{2,1,0:T(8,128)(2,1)S(1)}, bf16[2,128,2048]{2,1,0:T(8,128)(2,1)S(1)}, u32[]{:S(2)}, u32[]{:S(2)}) collective-permute-start(bf16[2,128,2048]{2,1,0:T(8,128)(2,1)S(1)} %get-tuple-element.26), channel_id=1, source_target_pairs={{0,1},{1,0},{2,3},{3,2},{4,5},{5,4},{6,7},{7,6},{8,9},{9,8},{10,11... | collective-permute-start | bytes 3145736 | tf_op jit(solution)/shard_map/ppermute | solution.py:29
  71.7 3.5 %collective-permute-start.19 = (bf16[3,32,2176]{2,1,0:T(8,128)(2,1)S(1)}, bf16[3,32,2176]{2,1,0:T(8,128)(2,1)S(1)}, u32[]{:S(2)}, u32[]{:S(2)}) collective-permute-start(bf16[3,32,2176]{2,1,0:T(8,128)(2,1)S(1)} %join.1.refs_0_), channel_id=1, source_target_pairs={{0,1},{1,0},{2,3},{3,2},{4,5},{5,4},{6,7},{7,6},{8,9},{9,8},{10,11... | collective-permute-start | bytes 1253384 | tf_op jit(solution)/shard_map/ppermute | solution.py:29
  71.8 4.0 %collective-permute-start.20 = (bf16[3,32,2176]{2,1,0:T(8,128)(2,1)S(1)}, bf16[3,32,2176]{2,1,0:T(8,128)(2,1)S(1)}, u32[]{:S(2)}, u32[]{:S(2)}) collective-permute-start(bf16[3,32,2176]{2,1,0:T(8,128)(2,1)S(1)} %collective-permute-done.12.refs_1_), channel_id=1, source_target_pairs={{0,1},{1,0},{2,3},{3,2},{4,5},{5,4},{6,7},{7,6},{8,9},{9,8},{10,11... | collective-permute-start | bytes 1253384 | tf_op jit(solution)/shard_map/ppermute | solution.py:29
  73.2 12.6 %collective-permute-start.6 = (bf16[2,128,512]{2,1,0:T(8,128)(2,1)S(1)}, bf16[2,128,512]{2,1,0:T(8,128)(2,1)S(1)}, u32[]{:S(2)}, u32[]{:S(2)}) collective-permute-start(bf16[2,128,512]{2,1,0:T(8,128)(2,1)S(1)} %bitcast.82), channel_id=1, source_target_pairs={{0,2},{1,3},{2,0},{3,1},{4,6},{5,7},{6,4},{7,5},{8,10},{9,11},{10,... | collective-permute-start | bytes 786440 | tf_op jit(solution)/shard_map/ppermute | solution.py:29
  81.8 25.7 %collective-permute-start.21 = (bf16[2,384,512]{2,1,0:T(8,128)(2,1)S(1)}, bf16[2,384,512]{2,1,0:T(8,128)(2,1)S(1)}, u32[]{:S(2)}, u32[]{:S(2)}) collective-permute-start(bf16[2,384,512]{2,1,0:T(8,128)(2,1)S(1)} %get-tuple-element.40), channel_id=1, source_target_pairs={{0,1},{1,0},{2,3},{3,2},{4,5},{5,4},{6,7},{7,6},{8,9},{9,8},{10,11... | collective-permute-start | bytes 2359304 | tf_op jit(solution)/shard_map/ppermute | solution.py:29
  82.2 40.6 %collective-permute-start.2 = (bf16[128,2048]{1,0:T(8,128)(2,1)S(1)}, bf16[128,2048]{1,0:T(8,128)(2,1)S(1)}, u32[]{:S(2)}, u32[]{:S(2)}) collective-permute-start(bf16[128,2048]{1,0:T(8,128)(2,1)S(1)} %fusion.1), channel_id=1, source_target_pairs={{0,2},{1,3},{2,0},{3,1},{4,6},{5,7},{6,4},{7,5},{8,10},{9,11},{10,... | collective-permute-start | bytes 1572872 | tf_op jit(solution)/shard_map/ppermute | solution.py:29
  83.8 23.6 %collective-permute-start.23 = (bf16[2,128,512]{2,1,0:T(8,128)(2,1)S(1)}, bf16[2,128,512]{2,1,0:T(8,128)(2,1)S(1)}, u32[]{:S(2)}, u32[]{:S(2)}) collective-permute-start(bf16[2,128,512]{2,1,0:T(8,128)(2,1)S(1)} %fusion.4), channel_id=1, source_target_pairs={{0,2},{1,3},{2,0},{3,1},{4,6},{5,7},{6,4},{7,5},{8,10},{9,11},{10,... | collective-permute-start | bytes 786440 | tf_op jit(solution)/shard_map/ppermute | solution.py:29
  84.3 20.6 %collective-permute-start.28 = (bf16[1,128,512]{2,1,0:T(8,128)(2,1)S(1)}, bf16[1,128,512]{2,1,0:T(8,128)(2,1)S(1)}, u32[]{:S(2)}, u32[]{:S(2)}) collective-permute-start(bf16[1,128,512]{2,1,0:T(8,128)(2,1)S(1)} %fusion.12), channel_id=1, source_target_pairs={{0,2},{1,3},{2,0},{3,1},{4,6},{5,7},{6,4},{7,5},{8,10},{9,11},{10,... | collective-permute-start | bytes 393224 | tf_op jit(solution)/shard_map/ppermute | solution.py:29
  104.9 6.8 %collective-permute-start.29 = (bf16[1,128,512]{2,1,0:T(8,128)(2,1)S(1)}, bf16[1,128,512]{2,1,0:T(8,128)(2,1)S(1)}, u32[]{:S(2)}, u32[]{:S(2)}) collective-permute-start(bf16[1,128,512]{2,1,0:T(8,128)(2,1)S(1)} %fusion.10), channel_id=1, source_target_pairs={{0,4},{1,5},{2,6},{3,7},{4,0},{5,1},{6,2},{7,3},{8,12},{9,13},{10,... | collective-permute-start | bytes 393224 | tf_op jit(solution)/shard_map/ppermute | solution.py:29
  107.5 11.9 %collective-permute-start.24 = (bf16[2,128,512]{2,1,0:T(8,128)(2,1)S(1)}, bf16[2,128,512]{2,1,0:T(8,128)(2,1)S(1)}, u32[]{:S(2)}, u32[]{:S(2)}) collective-permute-start(bf16[2,128,512]{2,1,0:T(8,128)(2,1)S(1)} %fusion.2), channel_id=1, source_target_pairs={{0,4},{1,5},{2,6},{3,7},{4,0},{5,1},{6,2},{7,3},{8,12},{9,13},{10,... | collective-permute-start | bytes 786440 | tf_op jit(solution)/shard_map/ppermute | solution.py:29
  107.7 11.6 %collective-permute-start.22 = (bf16[2,128,512]{2,1,0:T(8,128)(2,1)S(1)}, bf16[2,128,512]{2,1,0:T(8,128)(2,1)S(1)}, u32[]{:S(2)}, u32[]{:S(2)}) collective-permute-start(bf16[2,128,512]{2,1,0:T(8,128)(2,1)S(1)} %fusion.5), channel_id=1, source_target_pairs={{0,2},{1,3},{2,0},{3,1},{4,6},{5,7},{6,4},{7,5},{8,10},{9,11},{10,... | collective-permute-start | bytes 786440 | tf_op jit(solution)/shard_map/ppermute | solution.py:29
  109.3 8.7 %collective-permute-start.27 = (bf16[1,128,512]{2,1,0:T(8,128)(2,1)S(1)}, bf16[1,128,512]{2,1,0:T(8,128)(2,1)S(1)}, u32[]{:S(2)}, u32[]{:S(2)}) collective-permute-start(bf16[1,128,512]{2,1,0:T(8,128)(2,1)S(1)} %fusion.13), channel_id=1, source_target_pairs={{0,2},{1,3},{2,0},{3,1},{4,6},{5,7},{6,4},{7,5},{8,10},{9,11},{10,... | collective-permute-start | bytes 393224 | tf_op jit(solution)/shard_map/ppermute | solution.py:29
  111.7 12.1 %collective-permute-start.7 = (bf16[128,512]{1,0:T(8,128)(2,1)S(1)}, bf16[128,512]{1,0:T(8,128)(2,1)S(1)}, u32[]{:S(2)}, u32[]{:S(2)}) collective-permute-start(bf16[128,512]{1,0:T(8,128)(2,1)S(1)} %slice_bitcast_fusion.2), channel_id=1, source_target_pairs={{0,4},{1,5},{2,6},{3,7},{4,0},{5,1},{6,2},{7,3},{8,12},{9,13},{10,... | collective-permute-start | bytes 393224 | tf_op jit(solution)/shard_map/ppermute | solution.py:29
  118.1 6.4 %collective-permute-start.30 = (bf16[128,512]{1,0:T(8,128)(2,1)S(1)}, bf16[128,512]{1,0:T(8,128)(2,1)S(1)}, u32[]{:S(2)}, u32[]{:S(2)}) collective-permute-start(bf16[128,512]{1,0:T(8,128)(2,1)S(1)} %fusion.14), channel_id=1, source_target_pairs={{0,8},{1,9},{2,10},{3,11},{4,12},{5,13},{6,14},{7,15},{8,0},{9,1},... | collective-permute-start | bytes 393224 | tf_op jit(solution)/shard_map/ppermute | solution.py:29
  119.5 11.2 %collective-permute-start.25 = (bf16[128,512]{1,0:T(8,128)(2,1)S(1)}, bf16[128,512]{1,0:T(8,128)(2,1)S(1)}, u32[]{:S(2)}, u32[]{:S(2)}) collective-permute-start(bf16[128,512]{1,0:T(8,128)(2,1)S(1)} %get-tuple-element.46), channel_id=1, source_target_pairs={{0,16},{1,17},{2,18},{3,19},{4,20},{5,21},{6,22},{7,23},{8,24},{9,... | collective-permute-start | bytes 393224 | tf_op jit(solution)/shard_map/ppermute | solution.py:29
  121.5 9.2 %collective-permute-start.26 = (bf16[128,512]{1,0:T(8,128)(2,1)S(1)}, bf16[128,512]{1,0:T(8,128)(2,1)S(1)}, u32[]{:S(2)}, u32[]{:S(2)}) collective-permute-start(bf16[128,512]{1,0:T(8,128)(2,1)S(1)} %get-tuple-element.47), channel_id=1, source_target_pairs={{0,24},{1,25},{2,26},{3,27},{4,28},{5,29},{6,30},{7,31},{8,16},{9,... | collective-permute-start | bytes 393224 | tf_op jit(solution)/shard_map/ppermute | solution.py:29
